TPU v7x, 32 devices: a whole 2x2x4 slice. The times are simulated.
32 devices in a mesh: sp: 8 (over z, y), tp: 4 (over x, core).
Axes of the slice: x: 2, y: 2, z: 4, core: 2. Of those that a mesh axis runs over, the one named last changes fastest.
Arguments:
- tokens: bfloat16 [8192, 2048], P('sp', 'tp'), may hold values from -16 to 16
- mix_gain: float32 [2048], replicated, may hold values from 0.1 to 1.9
- query_weight: bfloat16 [2048, 1024], P(None, 'tp'), may hold values from -0.125 to 0.125
- key_weight: bfloat16 [2048, 1024], P(None, 'tp'), may hold values from -0.125 to 0.125
- value_weight: bfloat16 [2048, 1024], P(None, 'tp'), may hold values from -0.125 to 0.125
- outer_gate_weight: bfloat16 [2048, 1024], P(None, 'tp'), may hold values from -0.125 to 0.125
- inner_gate_weight: bfloat16 [2048, 1024], P(None, 'tp'), may hold values from -0.125 to 0.125
- conv_input_weight: bfloat16 [2048, 1024], P(None, 'tp'), may hold values from -0.125 to 0.125
- query_gain: float32 [64], replicated, may hold values from 0.6 to 10
- key_gain: float32 [64], replicated, may hold values from 0.6 to 10
- gate_totals: float32 [8192, 16], P('sp', 'tp'), may hold values from -2048 to 0, as said below
- conv_taps: float32 [3, 1024], P(None, 'tp'), may hold values from -3 to 3
- attn_out_gain: float32 [1024], P('tp'), may hold values from 0.1 to 1.9
- conv_out_gain: float32 [1024], P('tp'), may hold values from 0.1 to 1.9
- attn_out_weight: bfloat16 [1024, 2048], P('tp'), may hold values from -0.125 to 0.125
- conv_out_weight: bfloat16 [1024, 2048], P('tp'), may hold values from -0.125 to 0.125
Outputs:
- mixed: bfloat16 [8192, 2048], P(('sp', 'tp'))
Inputs may be any that keep to these rules, and one draw needn't show every extreme that they name: `gate_totals`: in every head the values never rise from one position to the next.
All inputs are finite; a program needn't handle non-finite values.
Results may differ from a plain program's by a relative error of at most 0.015.
The roundings to bfloat16 on the way count: a program that leaves them out, or rounds other values in their place, can miss the bound.
Values may be sent and summed in bfloat16 or wider, within the bound.
A program may use at most 64 MiB of HBM per device.

v0:
```python
import jax
import jax.numpy as jnp
from jax import lax
from jax.sharding import PartitionSpec as P

NORM_EPSILON = 1e-06


def shifted(shard, axis, by):
    devices = lax.axis_size(axis)
    pairs = [(i, i + by) for i in range(devices) if 0 <= i + by < devices]
    return lax.ppermute(shard, axis, pairs)


def head_norm(values, head_dim, gain):
    row_count = values.shape[0]
    grouped = values.reshape(row_count, -1, head_dim)
    normed = grouped * lax.rsqrt(jnp.mean(grouped * grouped, axis=2, keepdims=True) + NORM_EPSILON)
    return (normed * gain.reshape(-1, head_dim)).reshape(row_count, -1)


def per_device(
    tokens,
    mix_gain,
    query_weight,
    key_weight,
    value_weight,
    outer_gate_weight,
    inner_gate_weight,
    conv_input_weight,
    query_gain,
    key_gain,
    gate_totals,
    conv_taps,
    attn_out_gain,
    conv_out_gain,
    attn_out_weight,
    conv_out_weight,
):
    row_count = tokens.shape[0]
    head_dim = query_gain.shape[0]
    attn_width = query_weight.shape[1]
    conv_width = outer_gate_weight.shape[1]
    head_count = attn_width // head_dim
    stacked = jnp.concatenate(
        [
            query_weight,
            key_weight,
            value_weight,
            outer_gate_weight,
            inner_gate_weight,
            conv_input_weight,
        ],
        axis=1,
    )
    widened = tokens.astype(jnp.float32)
    squares = lax.psum(jnp.sum(widened * widened, axis=1), "tp")
    scaled = (
        lax.all_gather(tokens, "tp", axis=1, tiled=True).astype(jnp.float32) * mix_gain
    ).astype(jnp.bfloat16)
    product = jnp.dot(scaled, stacked, preferred_element_type=jnp.float32)
    row_scale = lax.rsqrt(squares / mix_gain.shape[0] + NORM_EPSILON)[:, None]
    projected = product * row_scale
    queries = head_norm(projected[:, 0:attn_width], head_dim, query_gain).astype(jnp.bfloat16)
    key_rows = head_norm(projected[:, attn_width : 2 * attn_width], head_dim, key_gain).astype(
        jnp.bfloat16
    )
    value_rows = projected[:, 2 * attn_width : 3 * attn_width].astype(jnp.bfloat16)
    conv_base = 3 * attn_width
    proj_outer = projected[:, conv_base : conv_base + conv_width]
    proj_inner = projected[:, conv_base + conv_width : conv_base + 2 * conv_width]
    proj_input = projected[:, conv_base + 2 * conv_width : conv_base + 3 * conv_width]
    all_gates = lax.all_gather(gate_totals, "sp", axis=0, tiled=True)
    query_start = lax.axis_index("sp") * row_count
    sp_count = lax.axis_size("sp")
    sequence_length = sp_count * row_count
    key_positions = jnp.arange(row_count, dtype=jnp.int32)
    score_scale = head_dim ** (-0.5)
    groups = [(queries, gate_totals, query_start + key_positions)]
    groups = [
        (
            group_rows.reshape(group_rows.shape[0], head_count, head_dim),
            group_gates.T,
            group_positions,
        )
        for group_rows, group_gates, group_positions in groups
    ]

    def fold_block(carried, block_keys, block_values, key_start):
        keys_heads = block_keys.reshape(row_count, head_count, head_dim)
        values_heads = block_values.reshape(row_count, head_count, head_dim)
        results = []
        for group, current_state in zip(groups, carried):
            group_queries, group_gates, group_positions = group

            def compute(
                current,
                group_queries=group_queries,
                group_gates=group_gates,
                group_positions=group_positions,
            ):
                running_max, accum = current
                scores = (
                    jnp.einsum(
                        "qhd,khd->hqk",
                        group_queries,
                        keys_heads,
                        preferred_element_type=jnp.float32,
                    )
                    * score_scale
                )
                block_gates = lax.dynamic_slice_in_dim(all_gates, key_start, row_count, 0).T
                scores = scores + group_gates[:, :, None] - block_gates[:, None, :]
                allowed = (key_start + key_positions)[None, :] <= group_positions[:, None]
                new_max = jnp.maximum(
                    running_max, jnp.max(jnp.where(allowed[None], scores, -jnp.inf), axis=2)
                )
                weights = jnp.where(
                    allowed[None], jnp.exp(scores - new_max[:, :, None]), 0.0
                ).astype(jnp.bfloat16)
                factor = jnp.exp(running_max - new_max)
                added = jnp.einsum(
                    "hqk,khd->qhd", weights, values_heads, preferred_element_type=jnp.float32
                )
                return (new_max, accum * factor.T[:, :, None] + added)

            live = (key_start >= 0) & (key_start <= group_positions[-1])
            results.append(lax.cond(live, compute, lambda current: current, current_state))
        return tuple(results)

    initial = tuple(
        (
            (
                jnp.full((head_count, group[0].shape[0]), -1e30, jnp.float32),
                jnp.zeros((group[0].shape[0], head_count, head_dim), jnp.float32),
            )
            for group in groups
        )
    )
    start_at = jnp.int32(0)
    piece_keys = lax.all_gather(key_rows, "sp", axis=0, tiled=True)
    piece_values = lax.all_gather(value_rows, "sp", axis=0, tiled=True)

    def fold_one(block_number, current):
        offset = block_number * row_count
        block_keys = lax.dynamic_slice_in_dim(piece_keys, offset, row_count, 0)
        block_values = lax.dynamic_slice_in_dim(piece_values, offset, row_count, 0)
        key_start = jnp.mod(start_at + offset, sequence_length)
        return fold_block(current, block_keys, block_values, key_start)

    folded = lax.fori_loop(0, piece_keys.shape[0] // row_count, fold_one, initial)
    normed_groups = [
        head_norm(state[1].reshape(state[1].shape[0], attn_width), head_dim, attn_out_gain).astype(
            jnp.bfloat16
        )
        for state in folded
    ]
    attn_mixed = normed_groups[0]
    tap_count = conv_taps.shape[0]
    gated = (proj_inner * proj_input).astype(jnp.bfloat16)
    prior_rows = shifted(gated[row_count - tap_count + 1 :], "sp", 1)
    padded = jnp.concatenate([prior_rows, gated], axis=0).astype(jnp.float32)
    convolved = conv_taps[0] * padded[0:row_count]
    for tap_index in range(1, tap_count):
        convolved = convolved + conv_taps[tap_index] * padded[tap_index : tap_index + row_count]
    conv_mixed = head_norm(proj_outer * convolved, head_dim, conv_out_gain).astype(jnp.bfloat16)
    joined = jnp.concatenate([attn_mixed, conv_mixed], axis=1)
    out_weight = jnp.concatenate([attn_out_weight, conv_out_weight], axis=0)
    return lax.psum_scatter(
        jnp.dot(joined, out_weight, preferred_element_type=jnp.float32).astype(jnp.bfloat16),
        "tp",
        scatter_dimension=0,
        tiled=True,
    )


def solution(mesh):
    placed = (
        P("sp", "tp"),
        P(),
        P(None, "tp"),
        P(None, "tp"),
        P(None, "tp"),
        P(None, "tp"),
        P(None, "tp"),
        P(None, "tp"),
        P(),
        P(),
        P("sp", "tp"),
        P(None, "tp"),
        P("tp"),
        P("tp"),
        P("tp", None),
        P("tp", None),
    )
    return jax.shard_map(
        per_device, mesh=mesh, in_specs=placed, out_specs=P(("sp", "tp"), None), check_vma=False
    )
```

profile of v0, /device:TPU:0, one launch (start us, length us, event | category | flops | bytes accessed | tf_op | source)
XLA Modules:
  0.0 378.3 jit_solution(2975799271338801407)
XLA Ops:
  9.0 1.5 multiply_reduce_fusion
  10.5 8.4 %psum.7 = f32[1024]{0:T(1024)S(1)} all-reduce(f32[1024]{0:T(1024)S(1)} %multiply_reduce_fusion), channel_id=1, replica_groups=mesh['sp'=8,'tp'=4] {'tp'}, use_global_device_ids=true, to_apply=%region_1.0 | all-reduce | flops 1024 | bytes 8192 | tf_op jit(solution)/shard_map/psum | solution.py:57
  18.9 2.6 constant_dynamic-update-slice_fusion.5
  21.4 2.3 constant_dynamic-update-slice_fusion.4
  24.9 1.2 constant_dynamic-update-slice_fusion.2
  28.3 17.8 %all-gather.4.cloned.1.call-done = bf16[1024,2048]{1,0:T(8,128)(2,1)} async-done(((bf16[1024,512]{1,0:T(8,128)(2,1)}), bf16[1024,2048]{1,0:T(8,128)(2,1)}) %all-gather.4.cloned.1.call-update) | async-done | bytes 4194320 | tf_op jit(solution)/shard_map/all_gather | solution.py:59
  46.1 10.0 %convolution_multiply_fusion = f32[1024,1536]{1,0:T(8,128)S(1)} fusion(bf16[2048,1536]{1,0:T(8,128)(2,1)} %constant_dynamic-update-slice_fusion, bf16[1024,2048]{1,0:T(8,128)(2,1)} %all-gather.4.cloned.1.call-done, f32[2048]{0:T(1024)S(1)} %copy-done.10, f32[1024]{0:T(1024)S(1)} %add_rsqrt_fusion.4), kind=kOutput, calls=%fused_computation.21 | convolution fusion | flops 6450315264 | bytes 16789504 | tf_op jit(solution)/shard_map/dot_general | solution.py:61
  56.2 2.6 copy-done
  60.8 3.5 multiply_convert_fusion.4
  64.3 2.1 slice.97
  66.6 3.4 collective-permute-start
  70.0 31.5 %all_gather.14 = f32[8192,4]{0,1:T(4,128)S(1)} all-gather(f32[1024,4]{0,1:T(4,128)S(1)} %copy-done.6), channel_id=1, replica_groups=mesh['sp'=8,'tp'=4] {'sp'}, dimensions={0}, use_global_device_ids=true | all-gather | bytes 147456 | tf_op jit(solution)/shard_map/all_gather | solution.py:73
  102.7 1.6 fusion.29
  105.4 32.7 %all-gather.6.cloned.1.call-done = bf16[8192,256]{1,0:T(8,128)(2,1)} async-done(((bf16[1024,256]{1,0:T(8,128)(2,1)}), bf16[8192,256]{1,0:T(8,128)(2,1)}) %all-gather.6.cloned.1.call-update) | async-done | bytes 4194320 | tf_op jit(solution)/shard_map/all_gather | solution.py:141
  138.1 6.3 %copy.31 = bf16[8192,256]{0,1:T(8,128)(2,1)} copy(bf16[8192,256]{1,0:T(8,128)(2,1)} %all-gather.6.cloned.1.call-done) | data formatting | bytes 8388608
  144.5 67.1 %all-gather.8.cloned.1.call-done = bf16[8192,256]{1,0:T(8,128)(2,1)} async-done(((bf16[1024,256]{1,0:T(8,128)(2,1)}), bf16[8192,256]{1,0:T(8,128)(2,1)}) %all-gather.8.cloned.1.call-update) | async-done | bytes 4194320 | tf_op jit(solution)/shard_map/all_gather | solution.py:142
  211.6 6.4 %copy.32 = bf16[8192,256]{0,1:T(8,128)(2,1)} copy(bf16[8192,256]{1,0:T(8,128)(2,1)} %all-gather.8.cloned.1.call-done) | data formatting | bytes 8388608
  218.2 23.0 %while.18 = (s32[]{:T(128)}, f32[4,1024]{1,0:T(4,128)S(1)}, f32[1024,4,64]{0,2,1:T(8,128)S(1)}, s32[1024]{0:T(1024)S(1)}, bf16[8192,256]{0,1:T(8,128)(2,1)}, /*i...) while((s32[]{:T(128)}, f32[4,1024]{1,0:T(4,128)S(1)}, ...), condition=%wide.region_8.9_spmd.clone, body=%wide.region_4.8_spmd.clone.sunk | while | flops 1121457152 | bytes 42701296 | solution.py:151
  219.6 11.6 %conditional.3 = ((f32[4,1024]{1,0:T(4,128)S(1)}, f32[1024,4,64]{0,2,1:T(8,128)S(1)})) conditional(s32[]{:T(128)} %convert_element_type.80, (f32[4,1024]{1,0:T(4,128)S(1)}, f32[1024,4,64]{0,2,1:T(8,128)S(1)}) %tuple.67, (s32[]{:T(128)}, s32[1024]{0:T(1024)S(1)}, s32[1024]{0:T(1024)S(1)}, s32[]{:T(128)}, bf16[8192,256]{0,1:T(8,128)(2,1)}, ...), branch_computations={%region_5.5_spmd, %region_6.7_spmd} | conditional | flops 1121457152 | bytes 42696808 | solution.py:128
  219.7 1.3 constant_dynamic-slice_fusion
  221.6 4.6 %fusion.2 = (f32[4,1024]{1,0:T(4,128)S(1)}, f32[4,1024,1024]{2,1,0:T(8,128)S(1)}) fusion(f32[4,1024]{1,0:T(4,128)S(1)} %dynamic-slice_bitcast_fusion, f32[4,1024]{1,0:T(4,128)S(1)} %get-tuple-element.341, pred[1024,1024]{0,1:T(8,128)(4,1)S(1)} %broadcast_compare_fusion, bf16[1024,4,64]{0,2,1:T(8,128)(2,1)S(1)} %bitcast.49, ...), kind=kOutput, calls=%fused_computation.3 | convolution fusion | flops 557838336 | bytes 18923520 | tf_op jit(solution)/shard_map/while/body/eval_jaxpr/cond/branch_1_fun/qhd,khd->hqk/dot_general | solution.py:104
  226.2 4.9 %fusion.12 = f32[1024,4,64]{0,2,1:T(8,128)S(1)} fusion(bf16[1024,4,64]{0,2,1:T(8,128)(2,1)S(1)} %bitcast.48, f32[4,1024,1024]{2,1,0:T(8,128)S(1)} %get-tuple-element.423, f32[4,1024]{1,0:T(4,128)S(1)} %get-tuple-element.495, f32[4,1024]{1,0:T(4,128)S(1)} %dynamic-slice_bitcast_fusion, f32[4,1024]{1,0:T(4,128)S(1)} %get-tuple-element.341, ...), kind=kOutput, calls=%fused_computation.12 | convolution fusion | flops 562561024 | bytes 20512768 | tf_op jit(solution)/shard_map/while/body/eval_jaxpr/cond/branch_1_fun/hqk,khd->qhd/dot_general | solution.py:122
  241.6 5.8 %convolution_convert_fusion = bf16[1024,2048]{1,0:T(8,128)(2,1)} fusion(bf16[256,2048]{1,0:T(8,128)(2,1)} %param.35, bf16[256,2048]{1,0:T(8,128)(2,1)} %param.34, bf16[1024,256]{1,0:T(8,128)(2,1)S(1)} %multiply_convert_fusion.2, bf16[1024,256]{1,0:T(8,128)(2,1)S(1)} %copy.35), kind=kOutput, calls=%fused_computation.23 | convolution fusion | flops 2155872256 | bytes 7340032 | tf_op jit(solution)/shard_map/dot_general | solution.py:170
  247.5 124.3 %reduce-scatter.2.cloned.1.call-done = bf16[256,2048]{1,0:T(8,128)(2,1)} async-done(((bf16[1024,2048]{1,0:T(8,128)(2,1)}), bf16[256,2048]{1,0:T(8,128)(2,1)}) %reduce-scatter.2.cloned.1.call-update) | async-done | bytes 1048592 | tf_op jit(solution)/shard_map/reduce_scatter | solution.py:169
  (94 shorter events, 16.8 us)
Async XLA Ops:
  6.5 17.2 %copy-start.1 = (bf16[2048,256]{1,0:T(8,128)(2,1)S(1)}, bf16[2048,256]{1,0:T(8,128)(2,1)}, u32[]{:S(2)}) copy-start(bf16[2048,256]{1,0:T(8,128)(2,1)} %param.24) | copy-start | bytes 3145732
  6.5 18.4 %copy-start.2 = (bf16[2048,256]{1,0:T(8,128)(2,1)S(1)}, bf16[2048,256]{1,0:T(8,128)(2,1)}, u32[]{:S(2)}) copy-start(bf16[2048,256]{1,0:T(8,128)(2,1)} %param.25) | copy-start | bytes 3145732
  6.5 19.5 %copy-start.3 = (bf16[2048,256]{1,0:T(8,128)(2,1)S(1)}, bf16[2048,256]{1,0:T(8,128)(2,1)}, u32[]{:S(2)}) copy-start(bf16[2048,256]{1,0:T(8,128)(2,1)} %param.26) | copy-start | bytes 3145732
  6.5 39.6 %all-gather.4.cloned.1.call-start = ((), (), s32[]{:S(2)}) async-start(), calls=%async_computation.1 | async-start | bytes 5242880 | tf_op jit(solution)/shard_map/all_gather | solution.py:59
  7.3 130.9 %all-gather.6.cloned.1.call-start = ((), (), s32[]{:S(2)}) async-start(), calls=%async_computation.2 | async-start | bytes 4718592 | tf_op jit(solution)/shard_map/all_gather | solution.py:141
  18.8 8.3 %copy-start.4 = (bf16[2048,256]{1,0:T(8,128)(2,1)S(1)}, bf16[2048,256]{1,0:T(8,128)(2,1)}, u32[]{:S(2)}) copy-start(bf16[2048,256]{1,0:T(8,128)(2,1)} %param.27) | copy-start | bytes 3145732
  18.9 27.3 %copy-start.10 = (f32[2048]{0:T(1024)S(1)}, f32[2048]{0:T(1024)}, u32[]{:S(2)}) copy-start(f32[2048]{0:T(1024)} %param.21) | copy-start | bytes 24580
  56.1 2.7 copy-start
  60.4 6.1 %copy-start.7 = (f32[3,256]{1,0:T(4,128)S(1)}, f32[3,256]{1,0:T(4,128)}, u32[]{:S(2)}) copy-start(f32[3,256]{1,0:T(4,128)} %param.31) | copy-start | bytes 9220
  60.5 9.5 %copy-start.6 = (f32[1024,4]{0,1:T(4,128)S(1)}, f32[1024,4]{0,1:T(4,128)}, u32[]{:S(2)}) copy-start(f32[1024,4]{0,1:T(4,128)} %param.30) | copy-start | bytes 49156
  60.5 41.0 %copy-start.9 = (f32[256]{0:T(256)S(1)}, f32[256]{0:T(256)}, u32[]{:S(2)}) copy-start(f32[256]{0:T(256)} %param.32) | copy-start | bytes 3076
  64.3 147.3 %all-gather.8.cloned.1.call-start = ((), (), s32[]{:S(2)}) async-start(), calls=%async_computation.3 | async-start | bytes 4718592 | tf_op jit(solution)/shard_map/all_gather | solution.py:142
  66.5 305.3 %reduce-scatter.2.cloned.1.call-start = ((), (), s32[]{:S(2)}) async-start(), calls=%async_computation.4 | async-start | bytes 5242880 | tf_op jit(solution)/shard_map/reduce_scatter | solution.py:169
  66.6 36.0 %collective-permute-start = (bf16[2,256]{1,0:T(2,128)(2,1)S(1)}, bf16[2,256]{1,0:T(2,128)(2,1)S(1)}, u32[]{:S(2)}, u32[]{:S(2)}) collective-permute-start(bf16[2,256]{1,0:T(2,128)(2,1)S(1)} %slice.70), channel_id=1, source_target_pairs={{0,4},{4,8},{8,12},{12,16},{16,20},{20,24},{24,28},{1,5},{5,9},{9,... | collective-permute-start | bytes 3080 | tf_op jit(solution)/shard_map/ppermute | solution.py:12
  102.7 2.6 copy-start.8
  144.5 73.7 %copy-start.5 = (bf16[1024,256]{0,1:T(8,128)(2,1)S(1)}, bf16[1024,256]{0,1:T(8,128)(2,1)}, u32[]{:S(2)}) copy-start(bf16[1024,256]{0,1:T(8,128)(2,1)} %copy.30) | copy-start | bytes 1572868
Sparse Core Ops, SparseCore 0:
  8.9 37.1 all-gather.3
  64.4 73.6 all-gather.5
  140.3 71.3 all-gather.7
  247.6 124.1 reduce-scatter.1
where the time goes:
time: 379 us; the launch traced here: 378 us
  waiting for transfers between devices  243 us (64%)
  blocking collectives  39.9 us (11%)
  local copies, waits for them, and re-layouts  39 us (10%)
  matrix products  25.4 us (7%)
  between operations  13.4 us (4%)
  other arithmetic  8.24 us (2%)
  loops' own time  6.15 us (2%)
    reduce_scatter x1, waiting for transfers between devices, per_device(): lax.psum_scatter(jnp.dot(joined, out_weight, preferred_element_type=jnp.f...  124 us
    all_gather x1, waiting for transfers between devices, per_device(): piece_values = lax.all_gather(value_rows, 'sp', axis=0, tiled=True)  67.1 us
    all_gather x1, waiting for transfers between devices, per_device(): piece_keys = lax.all_gather(key_rows, 'sp', axis=0, tiled=True)  32.7 us
    all_gather x1, blocking collectives, per_device(): all_gates = lax.all_gather(gate_totals, 'sp', axis=0, tiled=True)  31.5 us
    unnamed x29, local copies, waits for them, and re-layouts  23.8 us
    all_gather x1, waiting for transfers between devices, per_device(): lax.all_gather(tokens, 'tp', axis=1, tiled=True).astype(jnp.float32)  17.8 us
    dot_general x1, matrix products, per_device(): product = jnp.dot(scaled, stacked, preferred_element_type=jnp.float32)  10 us
    psum x1, blocking collectives, per_device(): squares = lax.psum(jnp.sum(widened * widened, axis=1), 'tp')  8.38 us
  transfers between devices with their start and end apart: 5, of which 4 were waited for; matrix products, arithmetic and copies ran while one was open for 7% of the time, Pallas kernels for 0%

commit v1 on v0

v1 whole, which is shorter than its diff:
```python
import functools

import jax
import jax.numpy as jnp
from jax import lax
from jax.experimental import pallas as pl
from jax.experimental.pallas import tpu as pltpu
from jax.sharding import PartitionSpec as P

NORM_EPSILON = 1e-06
MESH = pl.DeviceIdType.MESH
CORES = 2
LANES = 128
VMEM = pltpu.VMEM


def head_norm(values, head_dim, gain):
    row_count = values.shape[0]
    grouped = values.reshape(row_count, -1, head_dim)
    normed = grouped * lax.rsqrt(jnp.mean(grouped * grouped, axis=2, keepdims=True) + NORM_EPSILON)
    return (normed * gain.reshape(-1, head_dim)).reshape(row_count, -1)


def greet(devices):
    barrier = pltpu.get_barrier_semaphore()
    for sp, tp in devices:
        pl.semaphore_signal(barrier, inc=1, device_id=(sp, tp), device_id_type=MESH)
    pl.semaphore_wait(barrier, len(devices))


def exchange_kernel(
    sp_count, head_count, block_ref, side_ref, out_ref, side_out, send, side_send, recv, side_recv,
    pass_send, pass_side_send, pass_recv, pass_side_recv, local
):
    sp = lax.axis_index("sp")
    tp = lax.axis_index("tp")
    core = lax.rem(tp, CORES)
    mate = tp + 1 - 2 * core
    targets = sp_count // CORES
    share = targets // head_count
    greet([(lax.rem(sp + step, sp_count), tp) for step in range(1, sp_count)] + [(sp, mate)])
    owner = core == sp // targets

    def copies(slot, head, target):
        return (
            pltpu.make_async_remote_copy(
                block_ref.at[head], out_ref.at[sp], send.at[slot], recv.at[sp],
                device_id=(target, tp), device_id_type=MESH,
            ),
            pltpu.make_async_remote_copy(
                side_ref.at[head], side_out.at[sp], side_send.at[slot], side_recv.at[sp],
                device_id=(target, tp), device_id_type=MESH,
            ),
        )

    def own(head):
        return (
            pltpu.make_async_copy(block_ref.at[head], out_ref.at[sp], local.at[0]),
            pltpu.make_async_copy(side_ref.at[head], side_out.at[sp], local.at[1]),
        )

    def plan(step):
        at = lax.rem(sp + 1 + step, targets)
        return at // share, core * targets + at

    for step in range(targets):
        head, target = plan(step)

        @pl.when(target != sp)
        def _():
            for copy in copies(step, head, target):
                copy.start()

        @pl.when(target == sp)
        def _():
            for copy in own(head):
                copy.start()

    def passed(source):
        return (
            pltpu.make_async_remote_copy(
                out_ref.at[source], out_ref.at[source], pass_send.at[source], pass_recv.at[source],
                device_id=(sp, mate), device_id_type=MESH,
            ),
            pltpu.make_async_remote_copy(
                side_out.at[source], side_out.at[source], pass_side_send.at[source],
                pass_side_recv.at[source], device_id=(sp, mate), device_id_type=MESH,
            ),
        )

    @pl.when(owner)
    def _():
        for step in range(sp_count):
            source = lax.rem(sp + step, sp_count)
            if step == 0:
                for copy in own(0):
                    copy.wait()
            else:
                pltpu.make_async_remote_copy(
                    block_ref.at[0], out_ref.at[source], send.at[0], recv.at[source],
                    device_id=(sp, mate), device_id_type=MESH,
                ).wait_recv()
                pltpu.make_async_remote_copy(
                    side_ref.at[0], side_out.at[source], side_send.at[0], side_recv.at[source],
                    device_id=(sp, mate), device_id_type=MESH,
                ).wait_recv()
            for copy in passed(source):
                copy.start()
        for step in range(sp_count):
            for copy in passed(lax.rem(sp + step, sp_count)):
                copy.wait_send()

    @pl.when(jnp.logical_not(owner))
    def _():
        for step in range(sp_count):
            for copy in passed(lax.rem(sp + step, sp_count)):
                copy.wait_recv()

    for step in range(targets):
        head, target = plan(step)

        @pl.when(target != sp)
        def _():
            for copy in copies(step, head, target):
                copy.wait_send()


def exchange(blocks, sides, sp_count):
    head_count = blocks.shape[0]
    targets = sp_count // CORES
    dma = pltpu.SemaphoreType.DMA
    return pl.pallas_call(
        functools.partial(exchange_kernel, sp_count, head_count),
        out_shape=(
            jax.ShapeDtypeStruct((sp_count,) + blocks.shape[1:], blocks.dtype),
            jax.ShapeDtypeStruct((sp_count,) + sides.shape[1:], sides.dtype),
        ),
        in_specs=[pl.BlockSpec(memory_space=VMEM)] * 2,
        out_specs=(pl.BlockSpec(memory_space=VMEM),) * 2,
        scratch_shapes=[
            dma((targets,)), dma((targets,)), dma((sp_count,)), dma((sp_count,)),
            dma((sp_count,)), dma((sp_count,)), dma((sp_count,)), dma((sp_count,)), dma((2,)),
        ],
        compiler_params=pltpu.CompilerParams(
            collective_id=0, has_side_effects=True, vmem_limit_bytes=48 * 1024 * 1024
        ),
    )(blocks, sides)


def giveback_kernel(sp_count, head_count, block_ref, out_ref, send, recv, local):
    sp = lax.axis_index("sp")
    tp = lax.axis_index("tp")
    core = lax.rem(tp, CORES)
    first = tp - core
    targets = sp_count // CORES
    greet(
        [
            (lax.rem(sp + step, sp_count), first + lax.rem(core + other, CORES))
            for step in range(sp_count)
            for other in range(CORES)
            if step or other
        ]
    )
    home = sp // targets
    slot = lax.rem(sp, targets) * CORES + core
    home_here = home == core
    for step in range(1, sp_count + 1):
        source = lax.rem(sp + step, sp_count)
        away = pltpu.make_async_remote_copy(
            block_ref.at[source], out_ref.at[slot], send.at[step - 1], recv.at[slot],
            device_id=(source, first + home), device_id_type=MESH,
        )
        if step < sp_count:
            away.start()
        else:

            @pl.when(home_here)
            def _():
                pltpu.make_async_copy(block_ref.at[source], out_ref.at[slot], local).start()

            @pl.when(jnp.logical_not(home_here))
            def _():
                away.start()

    for index in range(targets * CORES):
        giver = core * targets + index // CORES
        here = jnp.logical_and(giver == sp, core == index % CORES)

        @pl.when(here)
        def _():
            pltpu.make_async_copy(block_ref.at[0], out_ref.at[index], local).wait()

        @pl.when(jnp.logical_not(here))
        def _():
            pltpu.make_async_remote_copy(
                block_ref.at[0], out_ref.at[index], send.at[0], recv.at[index],
                device_id=(sp, tp + 1 - 2 * core), device_id_type=MESH,
            ).wait_recv()

    for step in range(1, sp_count + 1):
        source = lax.rem(sp + step, sp_count)
        away = pltpu.make_async_remote_copy(
            block_ref.at[source], out_ref.at[slot], send.at[step - 1], recv.at[slot],
            device_id=(source, first + home), device_id_type=MESH,
        )
        if step < sp_count:
            away.wait_send()
        else:

            @pl.when(jnp.logical_not(home_here))
            def _():
                away.wait_send()


def giveback(blocks, head_count):
    sp_count = blocks.shape[0]
    dma = pltpu.SemaphoreType.DMA
    return pl.pallas_call(
        functools.partial(giveback_kernel, sp_count, head_count),
        out_shape=jax.ShapeDtypeStruct((sp_count,) + blocks.shape[1:], blocks.dtype),
        in_specs=[pl.BlockSpec(memory_space=VMEM)],
        out_specs=pl.BlockSpec(memory_space=VMEM),
        scratch_shapes=[dma((sp_count,)), dma((sp_count,)), dma],
        compiler_params=pltpu.CompilerParams(
            collective_id=1, has_side_effects=True, vmem_limit_bytes=32 * 1024 * 1024
        ),
    )(blocks)


def attention_kernel(count_ref, query_ref, key_ref, kv_ref, gain_ref, out_ref):
    rows = query_ref.shape[1]
    width = gain_ref.shape[1]
    full = count_ref[pl.program_id(0)]
    queries = query_ref[0]

    def fold(index, carried, masked):
        top, total = carried
        at = pl.ds(pl.multiple_of(index * rows, rows), rows)
        scores = lax.dot_general(
            queries, key_ref[at, :], (((1,), (1,)), ((), ())), preferred_element_type=jnp.float32
        )
        if masked:
            row = lax.broadcasted_iota(jnp.int32, scores.shape, 0)
            column = lax.broadcasted_iota(jnp.int32, scores.shape, 1)
            scores = jnp.where(column <= row, scores, -jnp.inf)
        new_top = jnp.maximum(top, jnp.max(scores, axis=1, keepdims=True))
        weights = jnp.exp(scores - new_top).astype(jnp.bfloat16)
        added = jnp.dot(weights, kv_ref[at, :], preferred_element_type=jnp.float32)
        return new_top, total * jnp.exp(top - new_top) + added

    carried = (
        jnp.full((rows, 1), -1e30, jnp.float32),
        jnp.zeros((rows, kv_ref.shape[1]), jnp.float32),
    )
    carried = lax.fori_loop(0, full, lambda index, now: fold(index, now, False), carried)
    _, total = fold(full, carried, True)
    attended = total[:, width:]
    scale = lax.rsqrt(jnp.mean(attended * attended, axis=1, keepdims=True) + NORM_EPSILON)
    mixed = (attended * scale * gain_ref[...]).astype(jnp.bfloat16)
    out_ref[0] = jnp.concatenate([mixed[: rows // 2], mixed[rows // 2 :]], axis=1)


def attention(counts, queries, keys, kv, gain):
    sp_count, rows, _ = queries.shape
    return pl.pallas_call(
        attention_kernel,
        grid_spec=pltpu.PrefetchScalarGridSpec(
            num_scalar_prefetch=1,
            grid=(sp_count,),
            in_specs=[
                pl.BlockSpec((1, rows, queries.shape[2]), lambda i, n: (i, 0, 0)),
                pl.BlockSpec(keys.shape, lambda i, n: (0, 0)),
                pl.BlockSpec(kv.shape, lambda i, n: (0, 0)),
                pl.BlockSpec(gain.shape, lambda i, n: (0, 0)),
            ],
            out_specs=pl.BlockSpec((1, rows // 2, LANES), lambda i, n: (i, 0, 0)),
        ),
        out_shape=jax.ShapeDtypeStruct((sp_count, rows // 2, LANES), jnp.bfloat16),
        compiler_params=pltpu.CompilerParams(vmem_limit_bytes=48 * 1024 * 1024),
    )(counts, queries, keys, kv, gain)


def split_three(values):
    high = lax.reduce_precision(values, 8, 7)
    rest = values - high
    middle = lax.reduce_precision(rest, 8, 7)
    low = rest - middle
    return [part.astype(jnp.bfloat16) for part in (high, middle, low)]


def shifted(shard, axis, by):
    devices = lax.axis_size(axis)
    pairs = [(i, i + by) for i in range(devices) if 0 <= i + by < devices]
    return lax.ppermute(shard, axis, pairs)


def attend(queries, key_rows, value_rows, gate_totals, attn_out_gain, head_dim):
    rows, width = queries.shape
    heads = width // head_dim
    sp = lax.axis_index("sp")
    sp_count = lax.axis_size("sp")
    core = lax.rem(lax.axis_index("tp"), CORES)
    targets = sp_count // CORES
    share = targets // heads
    pieces = CORES * share
    piece = rows // pieces
    by_head = lambda array: array.reshape(rows, heads, head_dim).transpose(1, 0, 2)
    kv = jnp.concatenate([by_head(key_rows), by_head(value_rows)], axis=2)
    head_queries = by_head(queries)
    packed = jnp.concatenate([head_queries[:, : rows // 2], head_queries[:, rows // 2 :]], axis=2)
    blocks = jnp.concatenate([kv, packed], axis=1)
    gate_rows = gate_totals.T.reshape(heads, rows // LANES, LANES)
    gain_rows = jnp.pad(attn_out_gain.reshape(heads, 1, head_dim), ((0, 0), (0, 7), (0, LANES - head_dim)))
    sides = jnp.concatenate([gate_rows, gain_rows], axis=1)

    blocks, sides = exchange(blocks, sides, sp_count)

    gates = sides[:, : rows // LANES].reshape(sp_count * rows)
    gain = sides[0, rows // LANES : rows // LANES + 1, :head_dim]
    kv = blocks[:, :rows].reshape(sp_count * rows, 2 * head_dim)
    packed = blocks[:, rows:]
    unpacked = jnp.concatenate([packed[:, :, :head_dim], packed[:, :, head_dim:]], axis=1)
    place = lax.rem(sp, share) * CORES + core

    def pick(array):
        pairs = array.reshape((sp_count // 2, 2, pieces, piece) + array.shape[2:])
        even = lax.dynamic_index_in_dim(pairs[:, 0], place, 1, False)
        odd = lax.dynamic_index_in_dim(pairs[:, 1], pieces - 1 - place, 1, False)
        return jnp.stack([even, odd], axis=1).reshape((sp_count, piece) + array.shape[2:])

    mine = pick(unpacked)
    mine_gates = pick(gates.reshape(sp_count, rows))
    one = lambda array: jnp.ones(array.shape, jnp.bfloat16)
    extra = split_three(mine_gates)
    spare = 2 * head_dim - head_dim - 6
    query_side = jnp.concatenate(
        [(mine.astype(jnp.float32) * head_dim ** (-0.5)).astype(jnp.bfloat16)]
        + [jnp.stack(extra + [one(mine_gates)] * 3, axis=2)]
        + [jnp.zeros(mine_gates.shape + (spare,), jnp.bfloat16)],
        axis=2,
    )
    extra = split_three(-gates)
    key_side = jnp.concatenate(
        [kv[:, :head_dim], jnp.stack([one(gates)] * 3 + extra, axis=1)]
        + [jnp.zeros(gates.shape + (spare,), jnp.bfloat16)],
        axis=1,
    )
    source = jnp.arange(sp_count, dtype=jnp.int32)
    counts = source * pieces + jnp.where(source % 2 == 0, place, pieces - 1 - place)
    finished = attention(counts.astype(jnp.int32), query_side, key_side, kv, gain)

    back = giveback(finished, heads)
    back = back.reshape(heads, pieces, piece // 2, 2, head_dim)
    back = jnp.where(sp % 2 == 0, back, back[:, ::-1])
    return back.transpose(1, 3, 2, 0, 4).reshape(rows, width)


def per_device(
    tokens,
    mix_gain,
    query_weight,
    key_weight,
    value_weight,
    outer_gate_weight,
    inner_gate_weight,
    conv_input_weight,
    query_gain,
    key_gain,
    gate_totals,
    conv_taps,
    attn_out_gain,
    conv_out_gain,
    attn_out_weight,
    conv_out_weight,
):
    row_count = tokens.shape[0]
    head_dim = query_gain.shape[0]
    gathered = lax.all_gather(tokens, "tp", axis=1, tiled=True).astype(jnp.float32)
    squares = jnp.sum(gathered * gathered, axis=1)
    scaled = (gathered * mix_gain).astype(jnp.bfloat16)
    row_scale = lax.rsqrt(squares / mix_gain.shape[0] + NORM_EPSILON)[:, None]

    def project(weight):
        return jnp.dot(scaled, weight, preferred_element_type=jnp.float32) * row_scale

    queries = head_norm(project(query_weight), head_dim, query_gain).astype(jnp.bfloat16)
    key_rows = head_norm(project(key_weight), head_dim, key_gain).astype(jnp.bfloat16)
    value_rows = project(value_weight).astype(jnp.bfloat16)
    proj_outer = project(outer_gate_weight)
    gated = (project(inner_gate_weight) * project(conv_input_weight)).astype(jnp.bfloat16)
    attn_mixed = attend(queries, key_rows, value_rows, gate_totals, attn_out_gain, head_dim)
    tap_count = conv_taps.shape[0]
    prior_rows = shifted(gated[row_count - tap_count + 1 :], "sp", 1)
    padded = jnp.concatenate([prior_rows, gated], axis=0).astype(jnp.float32)
    convolved = conv_taps[0] * padded[0:row_count]
    for tap_index in range(1, tap_count):
        convolved = convolved + conv_taps[tap_index] * padded[tap_index : tap_index + row_count]
    conv_mixed = head_norm(proj_outer * convolved, head_dim, conv_out_gain).astype(jnp.bfloat16)
    partial = jnp.dot(attn_mixed, attn_out_weight, preferred_element_type=jnp.float32)
    partial = partial + jnp.dot(conv_mixed, conv_out_weight, preferred_element_type=jnp.float32)
    return lax.psum_scatter(partial.astype(jnp.bfloat16), "tp", scatter_dimension=0, tiled=True)


def solution(mesh):
    placed = (
        P("sp", "tp"),
        P(),
        P(None, "tp"),
        P(None, "tp"),
        P(None, "tp"),
        P(None, "tp"),
        P(None, "tp"),
        P(None, "tp"),
        P(),
        P(),
        P("sp", "tp"),
        P(None, "tp"),
        P("tp"),
        P("tp"),
        P("tp", None),
        P("tp", None),
    )
    return jax.shard_map(
        per_device, mesh=mesh, in_specs=placed, out_specs=P(("sp", "tp"), None), check_vma=False
    )
```

time: 379 us -> 303 us (0.80)
  waiting for transfers between devices: 243 us -> 85 us
  Pallas kernels: 0 us -> 102 us
  blocking collectives: 39.9 us -> 0 us
  local copies, waits for them, and re-layouts: 39 us -> 62.9 us
  other arithmetic: 8.24 us -> 14.8 us
  loops' own time: 6.15 us -> 0 us
  matrix products: 25.4 us -> 20.1 us
    pallas_call x0 -> x3, Pallas kernels: none -> 102 us  [the longest x1 47.5 us: attention(): pl.pallas_call(attention_kernel, grid_spec=pltpu.PrefetchScalarGridSpec(n...]
    all_gather x2 -> x0, waiting for transfers between devices: 99.8 us -> none  [the longest x1 67.1 us: per_device(): piece_values = lax.all_gather(value_rows, 'sp', axis=0, tiled=True)]
    reduce_scatter x1, waiting for transfers between devices: 124 us -> 48.7 us  [per_device(): lax.psum_scatter(partial.astype(jnp.bfloat16), 'tp', scatter_dimension=0,...]
    all_gather x1 -> x0, blocking collectives: 31.5 us -> none  [per_device(): all_gates = lax.all_gather(gate_totals, 'sp', axis=0, tiled=True)]
    concatenate x1 -> x4, local copies, waits for them, and re-layouts: 1.13 us -> 24 us  [the longest x2 15.2 us: attend(): jnp.concatenate([kv[:, :head_dim], jnp.stack([one(gates)] * 3 + extra, ax...]
    all_gather x1, waiting for transfers between devices: 17.8 us -> 35 us  [per_device(): lax.all_gather(tokens, 'tp', axis=1, tiled=True).astype(jnp.float32)]
    unnamed x29 -> x37, local copies, waits for them, and re-layouts: 23.8 us -> 8.6 us
    psum x1 -> x0, blocking collectives: 8.38 us -> none  [per_device(): squares = lax.psum(jnp.sum(widened * widened, axis=1), 'tp')]
  transfers between devices with their start and end apart: 5 -> 3, of which waited for: 4 -> 3; matrix products, arithmetic and copies ran while one was open for 7% -> 2% of each run, Pallas kernels for 0% -> 0%
where the time goes in v1:
time: 303 us; the launch traced here: 302 us
  Pallas kernels  102 us (34%)
  waiting for transfers between devices  85 us (28%)
  local copies, waits for them, and re-layouts  62.9 us (21%)
  matrix products  20.1 us (7%)
  other arithmetic  14.8 us (5%)
  between operations  13.8 us (5%)
  starting transfers between devices  3.55 us (1%)
    reduce_scatter x1, waiting for transfers between devices, per_device(): lax.psum_scatter(partial.astype(jnp.bfloat16), 'tp', scatter_dimension=0,...  48.7 us
    pallas_call x1, Pallas kernels, attention(): pl.pallas_call(attention_kernel, grid_spec=pltpu.PrefetchScalarGridSpec(n...  47.5 us
    pallas_call x1, Pallas kernels, exchange(): pl.pallas_call(functools.partial(exchange_kernel, sp_count, head_count),...  44.4 us
    all_gather x1, waiting for transfers between devices, per_device(): lax.all_gather(tokens, 'tp', axis=1, tiled=True).astype(jnp.float32)  35 us
    dot_general x6, matrix products, project(): jnp.dot(scaled, weight, preferred_element_type=jnp.float32) * row_scale  15.5 us
    concatenate x2, local copies, waits for them, and re-layouts, attend(): jnp.concatenate([kv[:, :head_dim], jnp.stack([one(gates)] * 3 + extra, ax...  15.2 us
    pallas_call x1, Pallas kernels, giveback(): pl.pallas_call(functools.partial(giveback_kernel, sp_count, head_count),...  10.5 us
    concatenate x2, local copies, waits for them, and re-layouts, attend(): jnp.concatenate([(mine.astype(jnp.float32) * head_dim ** (-0.5)).astype(j...  8.83 us
  transfers between devices with their start and end apart: 3, of which 3 were waited for; matrix products, arithmetic and copies ran while one was open for 2% of the time, Pallas kernels for 0%

profile of v1, /device:TPU:0, one launch (start us, length us, event | category | flops | bytes accessed | tf_op | source)
XLA Modules:
  0.0 302.5 jit_solution(8998984878393664634)
XLA Ops:
  11.1 35.0 %all-gather.2.cloned.1.call-done = bf16[1024,2048]{1,0:T(8,128)(2,1)} async-done(((bf16[1024,512]{1,0:T(8,128)(2,1)}), bf16[1024,2048]{1,0:T(8,128)(2,1)}) %all-gather.2.cloned.1.call-update) | async-done | bytes 4194320 | tf_op jit(solution)/shard_map/all_gather | solution.py:378
  46.1 3.2 %fusion.1 = f32[1024]{0:T(1024)S(1)} fusion(bf16[1024,2048]{1,0:T(8,128)(2,1)} %all-gather.2.cloned.1.call-done), kind=kLoop, calls=%fused_computation.3 | loop fusion | flops 6290432 | bytes 4198400 | tf_op jit(solution)/shard_map/reduce_sum | solution.py:379
  52.5 3.8 %bitcast_reduce_fusion.2 = (f32[1024,4]{0,1:T(4,128)S(1)}, f32[1024,256]{0,1:T(8,128)S(1)}) fusion(f32[1024]{0:T(1024)S(1)} %add_rsqrt_fusion.3, bf16[2048,256]{1,0:T(8,128)(2,1)} %param.19, bf16[1024,2048]{1,0:T(8,128)(2,1)} %all-gather.2.cloned.1.call-done, f32[2048]{0:T(1024)S(1)} %copy-done.17), kind=kOutput, calls=%fused_computation.46 | convolution fusion | flops 1080815616 | bytes 6320128 | tf_op jit(solution)/shard_map/dot_general | solution.py:384
  57.8 3.8 %fusion.43 = bf16[1024,256]{0,1:T(8,128)(2,1)S(1)} fusion(bf16[2048,256]{1,0:T(8,128)(2,1)} %param.20, bf16[1024,2048]{1,0:T(8,128)(2,1)} %all-gather.2.cloned.1.call-done, f32[2048]{0:T(1024)S(1)} %copy-done.17, f32[1024]{0:T(1024)S(1)} %add_rsqrt_fusion.3), kind=kOutput, calls=%fused_computation.29 | convolution fusion | flops 1080557568 | bytes 5779456 | tf_op jit(solution)/shard_map/dot_general | solution.py:384
  62.9 2.6 maximum_maximum_fusion.block_ref
  65.5 44.4 %shard_map.154 = (bf16[8,1536,128]{2,1,0:T(8,128)(2,1)S(1)}, f32[8,16,128]{2,1,0:T(8,128)S(1)}) custom-call(bf16[4,1536,128]{2,1,0:T(8,128)(2,1)S(1)} %maximum_maximum_fusion.block_ref, f32[4,16,128]{2,1,0:T(8,128)S(1)} %select_maximum_fusion.side_ref), custom_call_target="tpu_custom_call" | custom-call | tf_op jit(solution)/shard_map/pallas_call | solution.py:132
  111.7 2.7 copy.36
  114.5 2.0 copy.33
  116.5 1.9 slice.69
  119.0 1.7 fusion.56
  120.7 2.6 copy.37
  123.3 1.8 copy.38
  125.2 2.0 copy.34
  128.6 2.1 pad_maximum_fusion
  132.7 2.8 fusion.2
  136.1 1.9 fusion.3
  144.1 13.6 %concatenate.38.key_ref = bf16[8192,128]{1,0:T(8,128)(2,1)} concatenate(bf16[8192,64]{1,0:T(8,128)(2,1)S(1)} %bitcast.68, bf16[8192,1]{1,0:T(8,128)(2,1)} %stack_broadcast_in_dim.7, bf16[8192,2]{1,0:T(8,128)(2,1)} %concatenate.37, bf16[8192,1]{1,0:T(8,128)(2,1)} %copy.38, bf16[8192,1]{1,0:T(8,128)(2,1)} %get-tuple-element.10, bf16[8192,1]{1,0:T(8,128)(2,1)} %get-tuple-element.9, ...), dimensions={1} | concatenate | bytes 4194304 | tf_op jit(solution)/shard_map/concatenate | solution.py:343
  161.2 7.6 %concatenate.36.query_ref = bf16[8,512,128]{2,1,0:T(8,128)(2,1)} concatenate(bf16[8,512,64]{2,1,0:T(8,128)(2,1)} %bitcast.74, bf16[8,512,1]{2,1,0:T(8,128)(2,1)} %copy.35, bf16[8,512,1]{2,1,0:T(8,128)(2,1)} %get-tuple-element.12, bf16[8,512,1]{2,1,0:T(8,128)(2,1)} %get-tuple-element.11, bf16[8,512,1]{2,1,0:T(8,128)(2,1)} %stack_broadcast_in_dim.6, ...), dimensions={2} | concatenate | bytes 2097152 | tf_op jit(solution)/shard_map/concatenate | solution.py:336
  171.7 47.5 %shard_map.155.block_ref = bf16[8,256,128]{2,1,0:T(8,128)(2,1)S(1)} custom-call(s32[8]{0:T(128)S(1)} %fusion.55.count_ref, bf16[8,512,128]{2,1,0:T(8,128)(2,1)S(1)} %copy-done.4, bf16[8192,128]{1,0:T(8,128)(2,1)S(1)} %copy-done.1, bf16[8192,128]{1,0:T(8,128)(2,1)S(1)} %bitcast.69, f32[1,64]{1,0:T(1,128)S(1)} %slice_bitcast_fusion.gain_ref), custom_call_target="tpu_custom_call" | custom-call | tf_op jit(solution)/shard_map/pallas_call | solution.py:265
  219.2 10.5 %shard_map.156 = bf16[8,256,128]{2,1,0:T(8,128)(2,1)S(1)} custom-call(bf16[8,256,128]{2,1,0:T(8,128)(2,1)S(1)} %shard_map.155.block_ref), custom_call_target="tpu_custom_call" | custom-call | tf_op jit(solution)/shard_map/pallas_call | solution.py:218
  230.9 3.6 %fusion.28 = f32[1024,256]{0,1:T(8,128)S(1)} fusion(bf16[2048,256]{1,0:T(8,128)(2,1)S(1)} %copy-done.14, bf16[1024,2048]{1,0:T(8,128)(2,1)} %all-gather.2.cloned.1.call-done, f32[2048]{0:T(1024)S(1)} %copy-done.17, f32[1024]{0:T(1024)S(1)} %add_rsqrt_fusion.3), kind=kOutput, calls=%fused_computation.24 | convolution fusion | flops 1080295424 | bytes 6303744 | tf_op jit(solution)/shard_map/dot_general | solution.py:384
  236.1 3.5 %collective-permute-start = (bf16[2,256]{0,1:T(8,128)(2,1)S(1)}, bf16[2,256]{0,1:T(8,128)(2,1)S(1)}, u32[]{:S(2)}, u32[]{:S(2)}) collective-permute-start(bf16[2,256]{0,1:T(8,128)(2,1)S(1)} %slice.86), channel_id=1, source_target_pairs={{0,4},{4,8},{8,12},{12,16},{16,20},{20,24},{24,28},{1,5},{5,9},{9,... | collective-permute-start | bytes 3080 | tf_op jit(solution)/shard_map/ppermute | solution.py:294
  243.7 3.3 %add_convert_fusion = bf16[1024,2048]{1,0:T(8,128)(2,1)} fusion(f32[1024,2048]{1,0:T(8,128)S(1)} %fusion.63, bf16[1024,256]{0,1:T(8,128)(2,1)S(1)} %fusion.49, bf16[256,2048]{1,0:T(8,128)(2,1)S(1)} %copy-done.11), kind=kOutput, calls=%fused_computation.4 | convolution fusion | flops 1077936128 | bytes 14155776 | tf_op jit(solution)/shard_map/dot_general | solution.py:400
  246.9 48.7 %reduce-scatter.2.cloned.1.call-done = bf16[256,2048]{1,0:T(8,128)(2,1)} async-done(((bf16[1024,2048]{1,0:T(8,128)(2,1)}), bf16[256,2048]{1,0:T(8,128)(2,1)}) %reduce-scatter.2.cloned.1.call-update) | async-done | bytes 1048592 | tf_op jit(solution)/shard_map/reduce_scatter | solution.py:401
  (90 shorter events, 36.1 us)
Async XLA Ops:
  6.5 233.1 %copy-start = (bf16[256,2048]{1,0:T(8,128)(2,1)S(1)}, bf16[256,2048]{1,0:T(8,128)(2,1)}, u32[]{:S(2)}) copy-start(bf16[256,2048]{1,0:T(8,128)(2,1)} %param.30) | copy-start | bytes 3145732
  6.5 42.8 %copy-start.17 = (f32[2048]{0:T(1024)S(1)}, f32[2048]{0:T(1024)}, u32[]{:S(2)}) copy-start(f32[2048]{0:T(1024)} %param.17) | copy-start | bytes 24580
  6.5 42.8 %copy-start.13 = (bf16[2048,256]{1,0:T(8,128)(2,1)S(1)}, bf16[2048,256]{1,0:T(8,128)(2,1)}, u32[]{:S(2)}) copy-start(bf16[2048,256]{1,0:T(8,128)(2,1)} %param.18) | copy-start | bytes 3145732
  6.5 39.6 %all-gather.2.cloned.1.call-start = ((), (), s32[]{:S(2)}) async-start(), calls=%async_computation.1 | async-start | bytes 5242880 | tf_op jit(solution)/shard_map/all_gather | solution.py:378
  7.3 288.4 %reduce-scatter.2.cloned.1.call-start = ((), (), s32[]{:S(2)}) async-start(), calls=%async_computation.2 | async-start | bytes 5242880 | tf_op jit(solution)/shard_map/reduce_scatter | solution.py:401
  46.1 3.4 %copy-start.9 = (bf16[1024,2048]{1,0:T(8,128)(2,1)S(1)}, bf16[1024,2048]{1,0:T(8,128)(2,1)}, u32[]{:S(2)}) copy-start(bf16[1024,2048]{1,0:T(8,128)(2,1)} %all-gather.2.cloned.1.call-done) | copy-start | bytes 12582916
  109.9 1.7 copy-start.2
  116.5 2.5 copy-start.3
  128.6 2.8 copy-start.5
  128.6 4.1 %copy-start.6 = (f32[8192,1]{1,0:T(8,128)S(1)}, f32[8192,1]{1,0:T(8,128)}, u32[]{:S(2)}) copy-start(f32[8192,1]{1,0:T(8,128)} %copy.37) | copy-start | bytes 98308
  132.6 2.8 copy-start.7
  132.6 3.4 %copy-start.8 = (f32[8,512,1]{2,1,0:T(8,128)S(1)}, f32[8,512,1]{2,1,0:T(8,128)}, u32[]{:S(2)}) copy-start(f32[8,512,1]{2,1,0:T(8,128)} %copy.34) | copy-start | bytes 49156
  168.9 1.6 copy-start.1
  170.4 1.2 copy-start.4
  219.1 11.8 %copy-start.14 = (bf16[2048,256]{1,0:T(8,128)(2,1)S(1)}, bf16[2048,256]{1,0:T(8,128)(2,1)}, u32[]{:S(2)}) copy-start(bf16[2048,256]{1,0:T(8,128)(2,1)} %param.22) | copy-start | bytes 3145732
  230.9 3.7 %copy-start.10 = (bf16[1024,2048]{1,0:T(8,128)(2,1)S(1)}, bf16[1024,2048]{1,0:T(8,128)(2,1)}, u32[]{:S(2)}) copy-start(bf16[1024,2048]{1,0:T(8,128)(2,1)} %all-gather.2.cloned.1.call-done) | copy-start | bytes 12582916
  230.9 3.7 %copy-start.15 = (bf16[2048,256]{1,0:T(8,128)(2,1)S(1)}, bf16[2048,256]{1,0:T(8,128)(2,1)}, u32[]{:S(2)}) copy-start(bf16[2048,256]{1,0:T(8,128)(2,1)} %param.23) | copy-start | bytes 3145732
  236.1 5.7 %copy-start.16 = (bf16[2048,256]{1,0:T(8,128)(2,1)S(1)}, bf16[2048,256]{1,0:T(8,128)(2,1)}, u32[]{:S(2)}) copy-start(bf16[2048,256]{1,0:T(8,128)(2,1)} %param.21) | copy-start | bytes 3145732
  236.1 5.4 %collective-permute-start = (bf16[2,256]{0,1:T(8,128)(2,1)S(1)}, bf16[2,256]{0,1:T(8,128)(2,1)S(1)}, u32[]{:S(2)}, u32[]{:S(2)}) collective-permute-start(bf16[2,256]{0,1:T(8,128)(2,1)S(1)} %slice.86), channel_id=1, source_target_pairs={{0,4},{4,8},{8,12},{12,16},{16,20},{20,24},{24,28},{1,5},{5,9},{9,... | collective-permute-start | bytes 3080 | tf_op jit(solution)/shard_map/ppermute | solution.py:294
  241.8 1.7 copy-start.12
  241.8 1.9 copy-start.11
Sparse Core Ops, SparseCore 0:
  8.9 37.1 all-gather.1
  247.1 48.5 reduce-scatter.1

commit v2 on v1

v2 whole, which is shorter than its diff:
```python
import functools

import jax
import jax.numpy as jnp
from jax import lax
from jax.experimental import pallas as pl
from jax.experimental.pallas import tpu as pltpu
from jax.sharding import PartitionSpec as P

NORM_EPSILON = 1e-06
MESH = pl.DeviceIdType.MESH
CORES = 2
LANES = 128
VMEM = pltpu.VMEM


def greet(devices):
    barrier = pltpu.get_barrier_semaphore()
    for sp, tp in devices:
        pl.semaphore_signal(barrier, inc=1, device_id=(sp, tp), device_id_type=MESH)
    pl.semaphore_wait(barrier, len(devices))


def mesh_copy(src, dst, send, recv, device):
    return pltpu.make_async_remote_copy(
        src, dst, send, recv, device_id=device, device_id_type=MESH
    )


def front_kernel(
    plan, tokens_ref, mix_ref, qkv_gain_ref, taps_ref, conv_gain_ref, side_ref, *refs
):
    sp_count, tp_count, head_count, head_dim, chunk = plan
    weight_refs = refs[:6]
    kv_out, query_out, side_out, conv_out = refs[6:10]
    (
        weights, gathered, scaled, kv_send, query_send, outer, padded, edge_send, edge_recv,
        weight_sem, own_sem, cross_send, mate_send, tok_pass_send, tok_recv,
        kv_ssem, kv_rsem, query_ssem, query_rsem, side_ssem, side_rsem,
        kv_psem, kv_prsem, query_psem, query_prsem, side_psem, side_prsem, local, edge_sem,
    ) = refs[10:]
    sp = lax.axis_index("sp")
    tp = lax.axis_index("tp")
    core = lax.rem(tp, CORES)
    mate = tp + 1 - 2 * core
    chips = tp_count // CORES
    targets = sp_count // CORES
    share = targets // head_count
    rows, features = tokens_ref.shape
    chunks = rows // chunk
    half = chunk // 2
    width = head_count * head_dim
    order = [chunks - 1] + list(range(chunks - 1))

    loads = [
        pltpu.make_async_copy(ref, weights.at[index], weight_sem.at[index])
        for index, ref in enumerate(weight_refs)
    ]
    for load in loads:
        load.start()
    mine = pltpu.make_async_copy(tokens_ref, gathered.at[tp], own_sem)
    mine.start()
    padded[0:8, :] = jnp.zeros((8, width), jnp.float32)
    greet(
        [(lax.rem(sp + step, sp_count), tp) for step in range(1, sp_count)]
        + [(sp, mate)]
        + [(sp, lax.rem(tp + CORES * step, tp_count)) for step in range(1, chips)]
    )

    def block(number):
        return pl.ds(number * chunk, chunk)

    def to_mate(number):
        return mesh_copy(
            tokens_ref.at[block(number)], gathered.at[tp, block(number)], mate_send.at[number],
            tok_recv.at[tp, number], (sp, mate),
        )

    def across(step, number):
        return mesh_copy(
            tokens_ref.at[block(number)], gathered.at[tp, block(number)],
            cross_send.at[step - 1, number], tok_recv.at[tp, number],
            (sp, lax.rem(tp + CORES * step, tp_count)),
        )

    def token_pass(step, number):
        other = lax.rem(tp + CORES * step, tp_count)
        return mesh_copy(
            gathered.at[other, block(number)], gathered.at[other, block(number)],
            tok_pass_send.at[step - 1, number], tok_recv.at[other, number], (sp, mate),
        )

    def token_arrival(source, number):
        return mesh_copy(
            tokens_ref.at[block(number)], gathered.at[source, block(number)], mate_send.at[number],
            tok_recv.at[source, number], (sp, mate),
        )

    for number in order:
        for step in range(1, chips):
            across(step, number).start()
        to_mate(number).start()

    owner = core == sp // targets

    def target_of(step):
        at = lax.rem(sp + 1 + step, targets)
        return at // share, core * targets + at

    def side_copy(step, head, target):
        return mesh_copy(
            side_ref.at[head], side_out.at[sp], side_ssem.at[step], side_rsem.at[sp], (target, tp)
        )

    def kv_copy(step, number, head, target):
        return mesh_copy(
            kv_send.at[head, block(number)], kv_out.at[sp, block(number)],
            kv_ssem.at[step, number], kv_rsem.at[sp, number], (target, tp),
        )

    def query_copy(step, number, head, target):
        at = pl.ds(number * half, half)
        return mesh_copy(
            query_send.at[head, at], query_out.at[sp, at],
            query_ssem.at[step, number], query_rsem.at[sp, number], (target, tp),
        )

    def kept(number, head):
        at = pl.ds(number * half, half)
        return (
            pltpu.make_async_copy(
                kv_send.at[head, block(number)], kv_out.at[sp, block(number)], local.at[0, number]
            ),
            pltpu.make_async_copy(
                query_send.at[head, at], query_out.at[sp, at], local.at[1, number]
            ),
        )

    def kept_side(head):
        return pltpu.make_async_copy(side_ref.at[head], side_out.at[sp], local.at[2, 0])

    for step in range(targets):
        head, target = target_of(step)

        @pl.when(target != sp)
        def _():
            side_copy(step, head, target).start()

        @pl.when(target == sp)
        def _():
            kept_side(head).start()

    ones_row = lax.broadcasted_iota(jnp.int32, (width, width), 0) // head_dim
    ones_column = lax.broadcasted_iota(jnp.int32, (width, width), 1) // head_dim
    spread = jnp.where(ones_row == ones_column, 1.0 / head_dim, 0.0).astype(jnp.bfloat16)

    def normed(values, gain):
        squares = values * values
        high = squares.astype(jnp.bfloat16)
        low = (squares - high.astype(jnp.float32)).astype(jnp.bfloat16)
        mean = jnp.dot(high, spread, preferred_element_type=jnp.float32)
        mean = mean + jnp.dot(low, spread, preferred_element_type=jnp.float32)
        return values * lax.rsqrt(mean + NORM_EPSILON) * gain

    mine.wait()
    for load in loads:
        load.wait()
    for number in order:
        here = block(number)
        for step in range(1, chips):
            token_arrival(lax.rem(tp + CORES * step, tp_count), number).wait_recv()
            token_pass(step, number).start()
        token_arrival(mate, number).wait_recv()
        for step in range(1, chips):
            token_arrival(lax.rem(mate + CORES * step, tp_count), number).wait_recv()
        total = jnp.zeros((chunk, 1), jnp.float32)
        for source in range(tp_count):
            part = gathered[source, here, :].astype(jnp.float32)
            at = slice(source * features, (source + 1) * features)
            total = total + jnp.sum(part * part, axis=1, keepdims=True)
            scaled[:, at] = (part * mix_ref[:, at]).astype(jnp.bfloat16)
        row_scale = lax.rsqrt(total / (tp_count * features) + NORM_EPSILON)

        def project(index):
            product = jnp.dot(scaled[...], weights[index], preferred_element_type=jnp.float32)
            return product * row_scale

        keys = normed(project(1), qkv_gain_ref[1:2, :]).astype(jnp.bfloat16)
        values = project(2).astype(jnp.bfloat16)
        queries = normed(project(0), qkv_gain_ref[0:1, :]).astype(jnp.bfloat16)
        queries = (queries.astype(jnp.float32) * head_dim ** (-0.5)).astype(jnp.bfloat16)
        for head in range(head_count):
            at = slice(head * head_dim, (head + 1) * head_dim)
            kv_send[head, here, :] = jnp.concatenate([keys[:, at], values[:, at]], axis=1)
            query_send[head, pl.ds(number * half, half), :] = jnp.concatenate(
                [queries[:half, at], queries[half:, at]], axis=1
            )
        for step in range(targets):
            head, target = target_of(step)

            @pl.when(target != sp)
            def _():
                kv_copy(step, number, head, target).start()
                query_copy(step, number, head, target).start()

            @pl.when(target == sp)
            def _():
                for copy in kept(number, head):
                    copy.start()

        outer[here, :] = project(3)
        gated = (project(4) * project(5)).astype(jnp.bfloat16)
        padded[pl.ds(8 + number * chunk, chunk), :] = gated.astype(jnp.float32)
        if number == chunks - 1:
            edge_send[...] = gated[chunk - 16 :, :]

            @pl.when(sp < sp_count - 1)
            def _():
                mesh_copy(
                    edge_send, edge_recv, edge_sem.at[0], edge_sem.at[1],
                    (lax.rem(sp + 1, sp_count), tp),
                ).start()

    edge = mesh_copy(
        edge_send, edge_recv, edge_sem.at[0], edge_sem.at[1], (lax.rem(sp + 1, sp_count), tp)
    )

    @pl.when(sp > 0)
    def _():
        edge.wait_recv()
        padded[0:8, :] = edge_recv[8:16, :].astype(jnp.float32)

    taps = taps_ref.shape[0]
    for number in range(chunks):
        convolved = jnp.zeros((chunk, width), jnp.float32)
        for tap in range(taps):
            at = pl.ds(8 - taps + 1 + tap + number * chunk, chunk)
            convolved = convolved + taps_ref[tap : tap + 1, :] * padded[at, :]
        conv_out[block(number), :] = normed(
            outer[block(number), :] * convolved, conv_gain_ref[...]
        ).astype(jnp.bfloat16)

    def kv_pass(source, number):
        return mesh_copy(
            kv_out.at[source, block(number)], kv_out.at[source, block(number)],
            kv_psem.at[source, number], kv_prsem.at[source, number], (sp, mate),
        )

    def query_pass(source, number):
        at = pl.ds(number * half, half)
        return mesh_copy(
            query_out.at[source, at], query_out.at[source, at],
            query_psem.at[source, number], query_prsem.at[source, number], (sp, mate),
        )

    def side_pass(source):
        return mesh_copy(
            side_out.at[source], side_out.at[source], side_psem.at[source], side_prsem.at[source],
            (sp, mate),
        )

    sources = [lax.rem(sp + step, sp_count) for step in range(sp_count)]

    @pl.when(owner)
    def _():
        for step, source in enumerate(sources):
            if step == 0:
                kept_side(0).wait()
            else:
                mesh_copy(
                    side_ref.at[0], side_out.at[source], side_ssem.at[0], side_rsem.at[source],
                    (sp, mate),
                ).wait_recv()
            side_pass(source).start()
        for number in order:
            at = pl.ds(number * half, half)
            for step, source in enumerate(sources):
                if step == 0:
                    for copy in kept(number, 0):
                        copy.wait()
                else:
                    mesh_copy(
                        kv_send.at[0, block(number)], kv_out.at[source, block(number)],
                        kv_ssem.at[0, number], kv_rsem.at[source, number], (sp, mate),
                    ).wait_recv()
                    mesh_copy(
                        query_send.at[0, at], query_out.at[source, at],
                        query_ssem.at[0, number], query_rsem.at[source, number], (sp, mate),
                    ).wait_recv()
                kv_pass(source, number).start()
                query_pass(source, number).start()
        for source in sources:
            side_pass(source).wait_send()
            for number in order:
                kv_pass(source, number).wait_send()
                query_pass(source, number).wait_send()

    @pl.when(jnp.logical_not(owner))
    def _():
        for source in sources:
            side_pass(source).wait_recv()
            for number in order:
                kv_pass(source, number).wait_recv()
                query_pass(source, number).wait_recv()

    for step in range(targets):
        head, target = target_of(step)

        @pl.when(target != sp)
        def _():
            side_copy(step, head, target).wait_send()
            for number in order:
                kv_copy(step, number, head, target).wait_send()
                query_copy(step, number, head, target).wait_send()

    for number in order:
        to_mate(number).wait_send()
        for step in range(1, chips):
            across(step, number).wait_send()
            token_pass(step, number).wait_send()

    @pl.when(sp < sp_count - 1)
    def _():
        edge.wait_send()


def front(tokens, mix_gain, qkv_gain, taps, conv_gain, sides, weights, head_dim, piece):
    sp_count = lax.axis_size("sp")
    tp_count = lax.axis_size("tp")
    rows, features = tokens.shape
    width = weights[0].shape[1]
    heads = width // head_dim
    chunk = min(256, piece)
    chunks = rows // chunk
    chips = tp_count // CORES
    targets = sp_count // CORES
    bf16 = jnp.bfloat16
    dma = pltpu.SemaphoreType.DMA
    across = (max(chips - 1, 1), chunks)
    vmem = pl.BlockSpec(memory_space=VMEM)
    return pl.pallas_call(
        functools.partial(front_kernel, (sp_count, tp_count, heads, head_dim, chunk)),
        out_shape=(
            jax.ShapeDtypeStruct((sp_count, rows, LANES), bf16),
            jax.ShapeDtypeStruct((sp_count, rows // 2, LANES), bf16),
            jax.ShapeDtypeStruct((sp_count,) + sides.shape[1:], sides.dtype),
            jax.ShapeDtypeStruct((rows, width), bf16),
        ),
        in_specs=[vmem] * 6 + [pl.BlockSpec(memory_space=pl.ANY)] * 6,
        out_specs=(vmem,) * 4,
        scratch_shapes=[
            VMEM((6,) + weights[0].shape, bf16),
            VMEM((tp_count, rows, features), bf16),
            VMEM((chunk, tp_count * features), bf16),
            VMEM((heads, rows, LANES), bf16),
            VMEM((heads, rows // 2, LANES), bf16),
            VMEM((rows, width), jnp.float32),
            VMEM((rows + 8, width), jnp.float32),
            VMEM((16, width), bf16),
            VMEM((16, width), bf16),
            dma((6,)), dma, dma(across), dma((chunks,)), dma(across), dma((tp_count, chunks)),
            dma((targets, chunks)), dma((sp_count, chunks)),
            dma((targets, chunks)), dma((sp_count, chunks)),
            dma((targets,)), dma((sp_count,)),
            dma((sp_count, chunks)), dma((sp_count, chunks)),
            dma((sp_count, chunks)), dma((sp_count, chunks)),
            dma((sp_count,)), dma((sp_count,)),
            dma((3, chunks)), dma((2,)),
        ],
        compiler_params=pltpu.CompilerParams(
            collective_id=0, has_side_effects=True, vmem_limit_bytes=56 * 1024 * 1024
        ),
    )(tokens, mix_gain, qkv_gain, taps, conv_gain, sides, *weights)


def giveback_kernel(sp_count, head_count, block_ref, out_ref, send, recv, local):
    sp = lax.axis_index("sp")
    tp = lax.axis_index("tp")
    core = lax.rem(tp, CORES)
    first = tp - core
    targets = sp_count // CORES
    greet(
        [
            (lax.rem(sp + step, sp_count), first + lax.rem(core + other, CORES))
            for step in range(sp_count)
            for other in range(CORES)
            if step or other
        ]
    )
    home = sp // targets
    slot = lax.rem(sp, targets) * CORES + core
    home_here = home == core
    for step in range(1, sp_count + 1):
        source = lax.rem(sp + step, sp_count)
        away = pltpu.make_async_remote_copy(
            block_ref.at[source], out_ref.at[slot], send.at[step - 1], recv.at[slot],
            device_id=(source, first + home), device_id_type=MESH,
        )
        if step < sp_count:
            away.start()
        else:

            @pl.when(home_here)
            def _():
                pltpu.make_async_copy(block_ref.at[source], out_ref.at[slot], local).start()

            @pl.when(jnp.logical_not(home_here))
            def _():
                away.start()

    for index in range(targets * CORES):
        giver = core * targets + index // CORES
        here = jnp.logical_and(giver == sp, core == index % CORES)

        @pl.when(here)
        def _():
            pltpu.make_async_copy(block_ref.at[0], out_ref.at[index], local).wait()

        @pl.when(jnp.logical_not(here))
        def _():
            pltpu.make_async_remote_copy(
                block_ref.at[0], out_ref.at[index], send.at[0], recv.at[index],
                device_id=(sp, tp + 1 - 2 * core), device_id_type=MESH,
            ).wait_recv()

    for step in range(1, sp_count + 1):
        source = lax.rem(sp + step, sp_count)
        away = pltpu.make_async_remote_copy(
            block_ref.at[source], out_ref.at[slot], send.at[step - 1], recv.at[slot],
            device_id=(source, first + home), device_id_type=MESH,
        )
        if step < sp_count:
            away.wait_send()
        else:

            @pl.when(jnp.logical_not(home_here))
            def _():
                away.wait_send()


def giveback(blocks, head_count):
    sp_count = blocks.shape[0]
    dma = pltpu.SemaphoreType.DMA
    return pl.pallas_call(
        functools.partial(giveback_kernel, sp_count, head_count),
        out_shape=jax.ShapeDtypeStruct((sp_count,) + blocks.shape[1:], blocks.dtype),
        in_specs=[pl.BlockSpec(memory_space=VMEM)],
        out_specs=pl.BlockSpec(memory_space=VMEM),
        scratch_shapes=[dma((sp_count,)), dma((sp_count,)), dma],
        compiler_params=pltpu.CompilerParams(
            collective_id=1, has_side_effects=True, vmem_limit_bytes=32 * 1024 * 1024
        ),
    )(blocks)


def attention_kernel(count_ref, query_ref, kv_ref, side_ref, out_ref):
    piece_rows = out_ref.shape[1] * 2
    head_dim = LANES // 2
    chunk_half = min(128, piece_rows // 2)
    full = count_ref[0, pl.program_id(0)]
    begin = pl.multiple_of(count_ref[1, pl.program_id(0)], chunk_half)
    side_rows = piece_rows // LANES
    rows = kv_ref.shape[1]
    per_source = rows // piece_rows
    low = lax.broadcasted_iota(jnp.int32, (chunk_half, LANES), 1) < head_dim
    tiles = []
    for number in range(piece_rows // (2 * chunk_half)):
        pair = query_ref[0, pl.ds(begin + number * chunk_half, chunk_half), :].astype(jnp.float32)
        left = jnp.where(low, pair, 0.0)
        right = jnp.where(low, pltpu.roll(pair, head_dim, 1), 0.0)
        tiles.append(jnp.concatenate([left, right], axis=0).astype(jnp.bfloat16))
    tile_rows = 2 * chunk_half

    def fold(index, carried, masked):
        source = index // per_source
        part = lax.rem(index, per_source)
        kv = kv_ref[source, pl.ds(pl.multiple_of(part * piece_rows, piece_rows), piece_rows), :]
        gates = side_ref[source, pl.ds(part * side_rows, side_rows), :]
        gate_row = jnp.concatenate([gates[row : row + 1, :] for row in range(side_rows)], axis=1)
        results = []
        for number, (top, total) in enumerate(carried):
            scores = lax.dot_general(
                tiles[number], kv, (((1,), (1,)), ((), ())), preferred_element_type=jnp.float32
            ) - gate_row
            if masked:
                row = lax.broadcasted_iota(jnp.int32, scores.shape, 0) + number * tile_rows
                column = lax.broadcasted_iota(jnp.int32, scores.shape, 1)
                scores = jnp.where(column <= row, scores, -jnp.inf)
            new_top = jnp.maximum(top, jnp.max(scores, axis=1, keepdims=True))
            weights = jnp.exp(scores - new_top).astype(jnp.bfloat16)
            added = jnp.dot(weights, kv, preferred_element_type=jnp.float32)
            results.append((new_top, total * jnp.exp(top - new_top) + added))
        return tuple(results)

    carried = tuple(
        (
            jnp.full((tile_rows, 1), -1e30, jnp.float32),
            jnp.zeros((tile_rows, LANES), jnp.float32),
        )
        for _ in tiles
    )
    carried = lax.fori_loop(0, full, lambda index, now: fold(index, now, False), carried)
    carried = fold(full, carried, True)
    gain = side_ref[0, rows // LANES : rows // LANES + 1, :head_dim]
    mixed = []
    for _, total in carried:
        attended = total[:, head_dim:]
        scale = lax.rsqrt(jnp.mean(attended * attended, axis=1, keepdims=True) + NORM_EPSILON)
        mixed.append((attended * scale * gain).astype(jnp.bfloat16))
    mixed = jnp.concatenate(mixed, axis=0)
    half = piece_rows // 2
    out_ref[0] = jnp.concatenate([mixed[:half], mixed[half:]], axis=1)


def attention(counts, queries, kv, sides, piece):
    sp_count = queries.shape[0]
    return pl.pallas_call(
        attention_kernel,
        grid_spec=pltpu.PrefetchScalarGridSpec(
            num_scalar_prefetch=1,
            grid=(sp_count,),
            in_specs=[
                pl.BlockSpec((1,) + queries.shape[1:], lambda i, n: (i, 0, 0)),
                pl.BlockSpec(kv.shape, lambda i, n: (0, 0, 0)),
                pl.BlockSpec(sides.shape, lambda i, n: (0, 0, 0)),
            ],
            out_specs=pl.BlockSpec((1, piece // 2, LANES), lambda i, n: (i, 0, 0)),
        ),
        out_shape=jax.ShapeDtypeStruct((sp_count, piece // 2, LANES), jnp.bfloat16),
        compiler_params=pltpu.CompilerParams(vmem_limit_bytes=48 * 1024 * 1024),
    )(counts, queries, kv, sides)


def per_device(
    tokens,
    mix_gain,
    query_weight,
    key_weight,
    value_weight,
    outer_gate_weight,
    inner_gate_weight,
    conv_input_weight,
    query_gain,
    key_gain,
    gate_totals,
    conv_taps,
    attn_out_gain,
    conv_out_gain,
    attn_out_weight,
    conv_out_weight,
):
    rows = tokens.shape[0]
    head_dim = query_gain.shape[0]
    width = query_weight.shape[1]
    heads = width // head_dim
    sp = lax.axis_index("sp")
    sp_count = lax.axis_size("sp")
    core = lax.rem(lax.axis_index("tp"), CORES)
    share = sp_count // CORES // heads
    pieces = CORES * share
    piece = rows // pieces
    gate_rows = gate_totals.T.reshape(heads, rows // LANES, LANES)
    gain_rows = jnp.pad(
        attn_out_gain.reshape(heads, 1, head_dim), ((0, 0), (0, 7), (0, LANES - head_dim))
    )
    sides = jnp.concatenate([gate_rows, gain_rows], axis=1)
    qkv_gain = jnp.stack([jnp.tile(query_gain, heads), jnp.tile(key_gain, heads)])
    kv, queries, sides, conv_mixed = front(
        tokens,
        mix_gain.reshape(1, -1),
        qkv_gain,
        conv_taps,
        conv_out_gain.reshape(1, -1),
        sides,
        (
            query_weight,
            key_weight,
            value_weight,
            outer_gate_weight,
            inner_gate_weight,
            conv_input_weight,
        ),
        head_dim,
        piece,
    )
    place = lax.rem(sp, share) * CORES + core
    source = jnp.arange(sp_count, dtype=jnp.int32)
    spot = jnp.where(source % 2 == 0, place, pieces - 1 - place)
    counts = jnp.stack([source * pieces + spot, spot * (piece // 2)]).astype(jnp.int32)
    finished = attention(counts, queries, kv, sides, piece)
    back = giveback(finished, heads)
    back = back.reshape(heads, pieces, piece // 2, 2, head_dim)
    back = jnp.where(sp % 2 == 0, back, back[:, ::-1])
    attn_mixed = back.transpose(1, 3, 2, 0, 4).reshape(rows, width)
    partial = jnp.dot(attn_mixed, attn_out_weight, preferred_element_type=jnp.float32)
    partial = partial + jnp.dot(conv_mixed, conv_out_weight, preferred_element_type=jnp.float32)
    return lax.psum_scatter(partial.astype(jnp.bfloat16), "tp", scatter_dimension=0, tiled=True)


def solution(mesh):
    placed = (
        P("sp", "tp"),
        P(),
        P(None, "tp"),
        P(None, "tp"),
        P(None, "tp"),
        P(None, "tp"),
        P(None, "tp"),
        P(None, "tp"),
        P(),
        P(),
        P("sp", "tp"),
        P(None, "tp"),
        P("tp"),
        P("tp"),
        P("tp", None),
        P("tp", None),
    )
    return jax.shard_map(
        per_device, mesh=mesh, in_specs=placed, out_specs=P(("sp", "tp"), None), check_vma=False
    )
```

time: 303 us -> 205 us (0.68)
  local copies, waits for them, and re-layouts: 62.9 us -> 7.83 us
  waiting for transfers between devices: 85 us -> 47.6 us
  Pallas kernels: 102 us -> 130 us
  matrix products: 20.1 us -> 4.61 us
  other arithmetic: 14.8 us -> 1.32 us
  starting transfers between devices: 3.55 us -> 0.01 us
    all_gather x1 -> x0, waiting for transfers between devices: 35 us -> none  [per_device(): lax.all_gather(tokens, 'tp', axis=1, tiled=True).astype(jnp.float32)]
    concatenate x4 -> x0, local copies, waits for them, and re-layouts: 24 us -> none  [the longest x2 15.2 us: attend(): jnp.concatenate([kv[:, :head_dim], jnp.stack([one(gates)] * 3 + extra, ax...]
    dot_general x6 -> x0, matrix products: 15.5 us -> none  [project(): jnp.dot(scaled, weight, preferred_element_type=jnp.float32) * row_scale]
    pallas_call x1, Pallas kernels: 44.4 us -> 59.5 us  [front(): pl.pallas_call(functools.partial(front_kernel, (sp_count, tp_count, heads...]
    pallas_call x1, Pallas kernels: 47.5 us -> 57.7 us  [attention(): pl.pallas_call(attention_kernel, grid_spec=pltpu.PrefetchScalarGridSpec(n...]
    convert_element_type x7 -> x0, other arithmetic: 6.7 us -> none  [the longest x2 4.7 us: split_three(): return [part.astype(jnp.bfloat16) for part in (high, middle, low)]]
    slice x7 -> x0, local copies, waits for them, and re-layouts: 5.53 us -> none  [the longest x1 1.89 us: attend(): kv = blocks[:, :rows].reshape(sp_count * rows, 2 * head_dim)]
    reshape x7 -> x2, local copies, waits for them, and re-layouts: 6.28 us -> 1.13 us  [the longest x1 0.76 us: per_device(): attn_out_gain.reshape(heads, 1, head_dim)]
  transfers between devices with their start and end apart: 3 -> 1, of which waited for: 3 -> 1; matrix products, arithmetic and copies ran while one was open for 2% -> 0% of each run, Pallas kernels for 0% -> 0%
where the time goes in v2:
time: 205 us
  Pallas kernels  130 us (63%)
  waiting for transfers between devices  47.6 us (23%)
  between operations  13.5 us (7%)
  local copies, waits for them, and re-layouts  7.83 us (4%)
  matrix products  4.61 us (2%)
    pallas_call x1, Pallas kernels, front(): pl.pallas_call(functools.partial(front_kernel, (sp_count, tp_count, heads...  59.5 us
    pallas_call x1, Pallas kernels, attention(): pl.pallas_call(attention_kernel, grid_spec=pltpu.PrefetchScalarGridSpec(n...  57.7 us
    reduce_scatter x1, waiting for transfers between devices, per_device(): lax.psum_scatter(partial.astype(jnp.bfloat16), 'tp', scatter_dimension=0,...  47.6 us
    pallas_call x1, Pallas kernels, giveback(): pl.pallas_call(functools.partial(giveback_kernel, sp_count, head_count),...  12.5 us
    unnamed x13, local copies, waits for them, and re-layouts  4.38 us
  transfers between devices with their start and end apart: 1, of which 1 were waited for; matrix products, arithmetic and copies ran while one was open for 0% of the time, Pallas kernels for 0%

profile of v2, /device:TPU:0, one launch (start us, length us, event | category | flops | bytes accessed | tf_op | source)
XLA Modules:
  0.0 204.6 jit_solution(378523619642330424)
XLA Ops:
  6.5 0.0 reduce-scatter.2.cloned.1.call-start
  6.5 0.7 tile.4
  7.3 0.1 stack_tile.6
  7.4 0.7 tile.5
  8.0 0.1 stack_tile.7
  8.1 0.8 reshape.64
  8.9 0.7 copy.21
  9.6 0.6 pad_maximum_fusion.qkv_gain_ref
  10.2 0.6 select_maximum_fusion.side_ref
  10.8 59.5 %shard_map.154 = (bf16[8,1024,128]{2,1,0:T(8,128)(2,1)}, bf16[8,512,128]{2,1,0:T(8,128)(2,1)}, f32[8,16,128]{2,1,0:T(8,128)}, bf16[1024,256]{1,0:T(8,128)(2,1)}) custom-call(bf16[1024,512]{1,0:T(8,128)(2,1)} %tokens_ref.1, f32[1,2048]{1,0:T(1,128)} %bitcast.19, f32[2,256]{1,0:T(2,128)} %pad_maximum_fusion.qkv_gain_ref, f32[3,256]{1,0:T(4,128)} %taps_ref.1, ...), custom_call_target="tpu_custom_call" | custom-call | tf_op jit(solution)/shard_map/pallas_call | solution.py:341
  70.4 1.6 copy-done.1
  72.0 1.2 copy-done.2
  73.2 0.8 copy-done.3
  74.0 57.7 %shard_map.155.block_ref = bf16[8,256,128]{2,1,0:T(8,128)(2,1)S(1)} custom-call(s32[2,8]{1,0:T(2,128)S(1)} %pad_add_fusion.count_ref, bf16[8,512,128]{2,1,0:T(8,128)(2,1)S(1)} %copy-done.2, bf16[8,1024,128]{2,1,0:T(8,128)(2,1)S(1)} %copy-done.1, f32[8,16,128]{2,1,0:T(8,128)S(1)} %copy-done.3), custom_call_target="tpu_custom_call" | custom-call | tf_op jit(solution)/shard_map/pallas_call | solution.py:517
  131.8 0.0 copy-start.4
  131.8 12.5 %shard_map.156 = bf16[8,256,128]{2,1,0:T(8,128)(2,1)S(1)} custom-call(bf16[8,256,128]{2,1,0:T(8,128)(2,1)S(1)} %shard_map.155.block_ref), custom_call_target="tpu_custom_call" | custom-call | tf_op jit(solution)/shard_map/pallas_call | solution.py:444
  144.3 0.2 copy.17
  144.5 0.1 fusion
  144.6 0.5 copy.18
  145.1 0.4 reshape.66
  145.5 1.3 fusion.1
  146.8 3.3 %add_convert_fusion = bf16[1024,2048]{1,0:T(8,128)(2,1)} fusion(f32[1024,2048]{1,0:T(8,128)S(1)} %fusion.1, bf16[1024,256]{1,0:T(8,128)(2,1)S(1)} %copy-done.5, bf16[256,2048]{1,0:T(8,128)(2,1)S(1)} %copy-done.4), kind=kOutput, calls=%fused_computation | convolution fusion | flops 1077936128 | bytes 14155776 | tf_op jit(solution)/shard_map/dot_general | solution.py:596
  150.2 0.0 reduce-scatter.2.cloned.1.call-update
  150.2 47.6 %reduce-scatter.2.cloned.1.call-done = bf16[256,2048]{1,0:T(8,128)(2,1)} async-done(((bf16[1024,2048]{1,0:T(8,128)(2,1)}), bf16[256,2048]{1,0:T(8,128)(2,1)}) %reduce-scatter.2.cloned.1.call-update) | async-done | bytes 1048592 | tf_op jit(solution)/shard_map/reduce_scatter | solution.py:597
  (10 shorter events, 0.0 us)
Async XLA Ops:
  6.5 139.0 %copy-start = (bf16[256,2048]{1,0:T(8,128)(2,1)S(1)}, bf16[256,2048]{1,0:T(8,128)(2,1)}, u32[]{:S(2)}) copy-start(bf16[256,2048]{1,0:T(8,128)(2,1)} %param.30) | copy-start | bytes 3145732
  6.5 191.2 %reduce-scatter.2.cloned.1.call-start = ((), (), s32[]{:S(2)}) async-start(), calls=%async_computation.1 | async-start | bytes 5242880 | tf_op jit(solution)/shard_map/reduce_scatter | solution.py:597
  70.4 1.6 copy-start.1
  72.0 1.2 copy-start.2
  73.2 0.8 copy-start.3
  131.8 15.0 %copy-start.4 = (bf16[256,2048]{1,0:T(8,128)(2,1)S(1)}, bf16[256,2048]{1,0:T(8,128)(2,1)}, u32[]{:S(2)}) copy-start(bf16[256,2048]{1,0:T(8,128)(2,1)} %param.31) | copy-start | bytes 3145732
  145.5 1.3 copy-start.5
Sparse Core Ops, SparseCore 0:
  150.3 47.3 reduce-scatter.1

commit v3 on v2

--- a/solution.py
+++ b/solution.py
@@ -373,12 +373,26 @@
     )(tokens, mix_gain, qkv_gain, taps, conv_gain, sides, *weights)
 
 
-def giveback_kernel(sp_count, head_count, block_ref, out_ref, send, recv, local):
+def back_kernel(
+    plan, done_ref, conv_ref, attn_weight, conv_weight, out_ref, landed, attn, partial, keep,
+    mate_out, mate_in, link_out, link_in, send, recv, local, mate_ssem, mate_rsem, link_ssem,
+    link_rsem
+):
+    sp_count, tp_count, head_dim, sub = plan
     sp = lax.axis_index("sp")
     tp = lax.axis_index("tp")
     core = lax.rem(tp, CORES)
+    mate = tp + 1 - 2 * core
+    chips = tp_count // CORES
     first = tp - core
     targets = sp_count // CORES
+    rows, width = conv_ref.shape
+    half = done_ref.shape[1]
+    piece = 2 * half
+    pieces = rows // piece
+    share = pieces // CORES
+    block_rows = rows // tp_count
+    subs = block_rows // sub
     greet(
         [
             (lax.rem(sp + step, sp_count), first + lax.rem(core + other, CORES))
@@ -386,27 +400,35 @@
             for other in range(CORES)
             if step or other
         ]
+        + [(sp, lax.rem(tp + CORES * step, tp_count)) for step in range(1, chips)]
     )
     home = sp // targets
     slot = lax.rem(sp, targets) * CORES + core
     home_here = home == core
-    for step in range(1, sp_count + 1):
+
+    def away(step):
         source = lax.rem(sp + step, sp_count)
-        away = pltpu.make_async_remote_copy(
-            block_ref.at[source], out_ref.at[slot], send.at[step - 1], recv.at[slot],
-            device_id=(source, first + home), device_id_type=MESH,
-        )
-        if step < sp_count:
-            away.start()
-        else:
-
-            @pl.when(home_here)
-            def _():
-                pltpu.make_async_copy(block_ref.at[source], out_ref.at[slot], local).start()
-
-            @pl.when(jnp.logical_not(home_here))
-            def _():
-                away.start()
+        return mesh_copy(
+            done_ref.at[source], landed.at[slot], send.at[step], recv.at[slot],
+            (source, first + home),
+        )
+
+    for step in range(1, sp_count):
+        away(step).start()
+
+    @pl.when(home_here)
+    def _():
+        pltpu.make_async_copy(done_ref.at[sp], landed.at[slot], local).start()
+
+    @pl.when(jnp.logical_not(home_here))
+    def _():
+        away(0).start()
+
+    for number in range(rows // block_rows):
+        at = pl.ds(number * block_rows, block_rows)
+        partial[at, :] = jnp.dot(
+            conv_ref[at, :], conv_weight[...], preferred_element_type=jnp.float32
+        )
 
     for index in range(targets * CORES):
         giver = core * targets + index // CORES
@@ -414,89 +436,171 @@
 
         @pl.when(here)
         def _():
-            pltpu.make_async_copy(block_ref.at[0], out_ref.at[index], local).wait()
+            pltpu.make_async_copy(done_ref.at[0], landed.at[index], local).wait()
 
         @pl.when(jnp.logical_not(here))
         def _():
-            pltpu.make_async_remote_copy(
-                block_ref.at[0], out_ref.at[index], send.at[0], recv.at[index],
-                device_id=(sp, tp + 1 - 2 * core), device_id_type=MESH,
+            mesh_copy(
+                done_ref.at[0], landed.at[index], send.at[0], recv.at[index], (sp, mate)
             ).wait_recv()
 
-    for step in range(1, sp_count + 1):
-        source = lax.rem(sp + step, sp_count)
-        away = pltpu.make_async_remote_copy(
-            block_ref.at[source], out_ref.at[slot], send.at[step - 1], recv.at[slot],
-            device_id=(source, first + home), device_id_type=MESH,
-        )
-        if step < sp_count:
-            away.wait_send()
-        else:
-
-            @pl.when(jnp.logical_not(home_here))
-            def _():
-                away.wait_send()
-
-
-def giveback(blocks, head_count):
-    sp_count = blocks.shape[0]
+        head = index // (share * CORES)
+        place = index % (share * CORES)
+        spot = jnp.where(lax.rem(sp, 2) == 0, place, pieces - 1 - place)
+        start = pl.multiple_of(spot * piece, piece)
+        lanes = slice(head * head_dim, (head + 1) * head_dim)
+        attn[pl.ds(start, half), lanes] = landed[index, :, :head_dim]
+        attn[pl.ds(start + half, half), lanes] = landed[index, :, head_dim:]
+
+    def product(block, number):
+        at = pl.ds(pl.multiple_of(block * block_rows + number * sub, sub), sub)
+        return partial[at, :] + jnp.dot(
+            attn[at, :], attn_weight[...], preferred_element_type=jnp.float32
+        )
+
+    def within(number):
+        return pl.ds(number * sub, sub)
+
+    def to_mate(step, number):
+        at = within(number)
+        return mesh_copy(
+            mate_out.at[step, at], mate_in.at[step, at], mate_ssem.at[step, number],
+            mate_rsem.at[step, number], (sp, mate),
+        )
+
+    def across(step, number):
+        at = within(number)
+        return mesh_copy(
+            link_out.at[step - 1, at], link_in.at[step - 1, at], link_ssem.at[step - 1, number],
+            link_rsem.at[step - 1, number], (sp, lax.rem(tp + CORES * step, tp_count)),
+        )
+
+    def joined(step, number):
+        at = within(number)
+        to_mate(step, number).wait_recv()
+        total = keep[step, at, :] + mate_in[step, at, :].astype(jnp.float32)
+        link_out[step - 1, at, :] = total.astype(jnp.bfloat16)
+        across(step, number).start()
+
+    waiting = []
+    for step in list(range(1, chips)) + [0]:
+        for number in range(subs):
+            at = within(number)
+            theirs = lax.rem(mate + CORES * step, tp_count)
+            ours = lax.rem(tp + CORES * step, tp_count)
+            mate_out[step, at, :] = product(theirs, number).astype(jnp.bfloat16)
+            to_mate(step, number).start()
+            keep[step, at, :] = product(ours, number)
+            if waiting:
+                joined(*waiting.pop())
+            if step:
+                waiting.append((step, number))
+    for number in range(subs):
+        at = within(number)
+        to_mate(0, number).wait_recv()
+        total = keep[0, at, :] + mate_in[0, at, :].astype(jnp.float32)
+        for step in range(1, chips):
+            across(step, number).wait_recv()
+            total = total + link_in[step - 1, at, :].astype(jnp.float32)
+        out_ref[at, :] = total.astype(jnp.bfloat16)
+    for step in range(chips):
+        for number in range(subs):
+            to_mate(step, number).wait_send()
+            if step:
+                across(step, number).wait_send()
+    for step in range(1, sp_count):
+        away(step).wait_send()
+
+    @pl.when(jnp.logical_not(home_here))
+    def _():
+        away(0).wait_send()
+
+
+def back(done, conv_mixed, attn_weight, conv_weight, head_dim):
+    sp_count = lax.axis_size("sp")
+    tp_count = lax.axis_size("tp")
+    chips = tp_count // CORES
+    rows, width = conv_mixed.shape
+    features = attn_weight.shape[1]
+    block_rows = rows // tp_count
+    sub = min(64, block_rows)
+    subs = block_rows // sub
+    links = max(chips - 1, 1)
+    bf16 = jnp.bfloat16
     dma = pltpu.SemaphoreType.DMA
+    vmem = pl.BlockSpec(memory_space=VMEM)
     return pl.pallas_call(
-        functools.partial(giveback_kernel, sp_count, head_count),
-        out_shape=jax.ShapeDtypeStruct((sp_count,) + blocks.shape[1:], blocks.dtype),
-        in_specs=[pl.BlockSpec(memory_space=VMEM)],
-        out_specs=pl.BlockSpec(memory_space=VMEM),
-        scratch_shapes=[dma((sp_count,)), dma((sp_count,)), dma],
+        functools.partial(back_kernel, (sp_count, tp_count, head_dim, sub)),
+        out_shape=jax.ShapeDtypeStruct((block_rows, features), bf16),
+        in_specs=[vmem] * 4,
+        out_specs=vmem,
+        scratch_shapes=[
+            VMEM(done.shape, bf16),
+            VMEM((rows, width), bf16),
+            VMEM((rows, features), jnp.float32),
+            VMEM((chips, block_rows, features), jnp.float32),
+            VMEM((chips, block_rows, features), bf16),
+            VMEM((chips, block_rows, features), bf16),
+            VMEM((links, block_rows, features), bf16),
+            VMEM((links, block_rows, features), bf16),
+            dma((sp_count,)), dma((sp_count,)), dma,
+            dma((chips, subs)), dma((chips, subs)), dma((links, subs)), dma((links, subs)),
+        ],
         compiler_params=pltpu.CompilerParams(
-            collective_id=1, has_side_effects=True, vmem_limit_bytes=32 * 1024 * 1024
+            collective_id=1, has_side_effects=True, vmem_limit_bytes=48 * 1024 * 1024
         ),
-    )(blocks)
-
-
-def attention_kernel(count_ref, query_ref, kv_ref, side_ref, out_ref):
+    )(done, conv_mixed, attn_weight, conv_weight)
+
+
+def attention_kernel(begin_ref, query_ref, kv_ref, side_ref, out_ref):
     piece_rows = out_ref.shape[1] * 2
     head_dim = LANES // 2
-    chunk_half = min(128, piece_rows // 2)
-    full = count_ref[0, pl.program_id(0)]
-    begin = pl.multiple_of(count_ref[1, pl.program_id(0)], chunk_half)
-    side_rows = piece_rows // LANES
+    tile = min(256, piece_rows)
+    half = tile // 2
+    sub = 256
+    full = pl.program_id(0)
+    begin = pl.multiple_of(begin_ref[full], half)
     rows = kv_ref.shape[1]
-    per_source = rows // piece_rows
-    low = lax.broadcasted_iota(jnp.int32, (chunk_half, LANES), 1) < head_dim
+    low = lax.broadcasted_iota(jnp.int32, (half, LANES), 1) < head_dim
     tiles = []
-    for number in range(piece_rows // (2 * chunk_half)):
-        pair = query_ref[0, pl.ds(begin + number * chunk_half, chunk_half), :].astype(jnp.float32)
+    for number in range(piece_rows // tile):
+        pair = query_ref[0, pl.ds(begin + number * half, half), :].astype(jnp.float32)
         left = jnp.where(low, pair, 0.0)
         right = jnp.where(low, pltpu.roll(pair, head_dim, 1), 0.0)
         tiles.append(jnp.concatenate([left, right], axis=0).astype(jnp.bfloat16))
-    tile_rows = 2 * chunk_half
-
-    def fold(index, carried, masked):
-        source = index // per_source
-        part = lax.rem(index, per_source)
-        kv = kv_ref[source, pl.ds(pl.multiple_of(part * piece_rows, piece_rows), piece_rows), :]
-        gates = side_ref[source, pl.ds(part * side_rows, side_rows), :]
-        gate_row = jnp.concatenate([gates[row : row + 1, :] for row in range(side_rows)], axis=1)
+
+    def fold(source, carried, masked):
         results = []
         for number, (top, total) in enumerate(carried):
-            scores = lax.dot_general(
-                tiles[number], kv, (((1,), (1,)), ((), ())), preferred_element_type=jnp.float32
-            ) - gate_row
-            if masked:
-                row = lax.broadcasted_iota(jnp.int32, scores.shape, 0) + number * tile_rows
-                column = lax.broadcasted_iota(jnp.int32, scores.shape, 1)
-                scores = jnp.where(column <= row, scores, -jnp.inf)
-            new_top = jnp.maximum(top, jnp.max(scores, axis=1, keepdims=True))
-            weights = jnp.exp(scores - new_top).astype(jnp.bfloat16)
-            added = jnp.dot(weights, kv, preferred_element_type=jnp.float32)
-            results.append((new_top, total * jnp.exp(top - new_top) + added))
+            scores = []
+            new_top = top
+            for start in range(0, rows, sub):
+                gates = side_ref[source, start // LANES : (start + sub) // LANES, :]
+                gate_row = jnp.concatenate(
+                    [gates[row : row + 1, :] for row in range(sub // LANES)], axis=1
+                )
+                part = lax.dot_general(
+                    tiles[number], kv_ref[source, start : start + sub, :],
+                    (((1,), (1,)), ((), ())), preferred_element_type=jnp.float32,
+                ) - gate_row
+                if masked:
+                    row = lax.broadcasted_iota(jnp.int32, part.shape, 0) + 2 * begin + number * tile
+                    column = lax.broadcasted_iota(jnp.int32, part.shape, 1) + start
+                    part = jnp.where(column <= row, part, -jnp.inf)
+                new_top = jnp.maximum(new_top, jnp.max(part, axis=1, keepdims=True))
+                scores.append(part)
+            total = total * jnp.exp(top - new_top)
+            for index, part in enumerate(scores):
+                weights = jnp.exp(part - new_top).astype(jnp.bfloat16)
+                total = total + jnp.dot(
+                    weights, kv_ref[source, index * sub : (index + 1) * sub, :],
+                    preferred_element_type=jnp.float32,
+                )
+            results.append((new_top, total))
         return tuple(results)
 
     carried = tuple(
-        (
-            jnp.full((tile_rows, 1), -1e30, jnp.float32),
-            jnp.zeros((tile_rows, LANES), jnp.float32),
-        )
+        (jnp.full((tile, 1), -1e30, jnp.float32), jnp.zeros((tile, LANES), jnp.float32))
         for _ in tiles
     )
     carried = lax.fori_loop(0, full, lambda index, now: fold(index, now, False), carried)
@@ -508,11 +612,11 @@
         scale = lax.rsqrt(jnp.mean(attended * attended, axis=1, keepdims=True) + NORM_EPSILON)
         mixed.append((attended * scale * gain).astype(jnp.bfloat16))
     mixed = jnp.concatenate(mixed, axis=0)
-    half = piece_rows // 2
-    out_ref[0] = jnp.concatenate([mixed[:half], mixed[half:]], axis=1)
-
-
-def attention(counts, queries, kv, sides, piece):
+    middle = piece_rows // 2
+    out_ref[0] = jnp.concatenate([mixed[:middle], mixed[middle:]], axis=1)
+
+
+def attention(begins, queries, kv, sides, piece):
     sp_count = queries.shape[0]
     return pl.pallas_call(
         attention_kernel,
@@ -528,7 +632,7 @@
         ),
         out_shape=jax.ShapeDtypeStruct((sp_count, piece // 2, LANES), jnp.bfloat16),
         compiler_params=pltpu.CompilerParams(vmem_limit_bytes=48 * 1024 * 1024),
-    )(counts, queries, kv, sides)
+    )(begins, queries, kv, sides)
 
 
 def per_device(
@@ -586,15 +690,9 @@
     place = lax.rem(sp, share) * CORES + core
     source = jnp.arange(sp_count, dtype=jnp.int32)
     spot = jnp.where(source % 2 == 0, place, pieces - 1 - place)
-    counts = jnp.stack([source * pieces + spot, spot * (piece // 2)]).astype(jnp.int32)
-    finished = attention(counts, queries, kv, sides, piece)
-    back = giveback(finished, heads)
-    back = back.reshape(heads, pieces, piece // 2, 2, head_dim)
-    back = jnp.where(sp % 2 == 0, back, back[:, ::-1])
-    attn_mixed = back.transpose(1, 3, 2, 0, 4).reshape(rows, width)
-    partial = jnp.dot(attn_mixed, attn_out_weight, preferred_element_type=jnp.float32)
-    partial = partial + jnp.dot(conv_mixed, conv_out_weight, preferred_element_type=jnp.float32)
-    return lax.psum_scatter(partial.astype(jnp.bfloat16), "tp", scatter_dimension=0, tiled=True)
+    begins = (spot * (piece // 2)).astype(jnp.int32)
+    finished = attention(begins, queries, kv, sides, piece)
+    return back(finished, conv_mixed, attn_out_weight, conv_out_weight, head_dim)
 
 
 def solution(mesh):

time: 205 us -> 151 us (0.74)
  waiting for transfers between devices: 47.6 us -> 0 us
  between operations: 13.5 us -> 0.07 us
  Pallas kernels: 130 us -> 141 us
  matrix products: 4.61 us -> 0 us
    reduce_scatter x1 -> x0, waiting for transfers between devices: 47.6 us -> none  [per_device(): lax.psum_scatter(partial.astype(jnp.bfloat16), 'tp', scatter_dimension=0,...]
    pallas_call x1, Pallas kernels: 12.5 us -> 38.8 us  [back(): pl.pallas_call(functools.partial(back_kernel, (sp_count, tp_count, head_d...]
    pallas_call x1, Pallas kernels: 57.7 us -> 42.1 us  [attention(): pl.pallas_call(attention_kernel, grid_spec=pltpu.PrefetchScalarGridSpec(n...]
    dot_general x2 -> x0, matrix products: 4.61 us -> none  [the longest x1 3.32 us: per_device(): jnp.dot(conv_mixed, conv_out_weight, preferred_element_type=jnp.float32)]
    unnamed x13 -> x14, local copies, waits for them, and re-layouts: 4.38 us -> 5.35 us
  transfers between devices with their start and end apart: 1 -> 0, of which waited for: 1 -> 0; matrix products, arithmetic and copies ran while one was open for 0% -> 0% of each run, Pallas kernels for 0% -> 0%
where the time goes in v3:
time: 151 us; the launch traced here: 149 us
  Pallas kernels  141 us (93%)
  local copies, waits for them, and re-layouts  7.59 us (5%)
    pallas_call x1, Pallas kernels, front(): pl.pallas_call(functools.partial(front_kernel, (sp_count, tp_count, heads...  59.7 us
    pallas_call x1, Pallas kernels, attention(): pl.pallas_call(attention_kernel, grid_spec=pltpu.PrefetchScalarGridSpec(n...  42.1 us
    pallas_call x1, Pallas kernels, back(): pl.pallas_call(functools.partial(back_kernel, (sp_count, tp_count, head_d...  38.8 us
    unnamed x14, local copies, waits for them, and re-layouts  5.35 us

profile of v3, /device:TPU:0, one launch (start us, length us, event | category | flops | bytes accessed | tf_op | source)
XLA Modules:
  0.0 149.5 jit_solution(2565508045377171667)
XLA Ops:
  0.0 0.7 tile.4
  0.7 0.1 stack_tile.6
  0.7 0.7 tile.5
  1.4 0.1 stack_tile.7
  1.5 0.6 pad_maximum_fusion.qkv_gain_ref
  2.1 0.8 reshape.17
  2.8 0.7 copy.19
  3.6 0.6 select_maximum_fusion.side_ref
  4.2 0.0 copy-start.1
  4.2 0.0 copy-start.2
  4.2 59.7 %shard_map.154 = (bf16[8,1024,128]{2,1,0:T(8,128)(2,1)}, bf16[8,512,128]{2,1,0:T(8,128)(2,1)}, f32[8,16,128]{2,1,0:T(8,128)}, bf16[1024,256]{1,0:T(8,128)(2,1)}) custom-call(bf16[1024,512]{1,0:T(8,128)(2,1)} %tokens_ref.1, f32[1,2048]{1,0:T(1,128)} %bitcast.9, f32[2,256]{1,0:T(2,128)} %pad_maximum_fusion.qkv_gain_ref, f32[3,256]{1,0:T(4,128)} %taps_ref.1, ...), custom_call_target="tpu_custom_call" | custom-call | tf_op jit(solution)/shard_map/pallas_call | solution.py:341
  63.9 0.0 copy-start
  63.9 1.6 %copy-done = bf16[8,1024,128]{2,1,0:T(8,128)(2,1)S(1)} copy-done((bf16[8,1024,128]{2,1,0:T(8,128)(2,1)S(1)}, bf16[8,1024,128]{2,1,0:T(8,128)(2,1)}, u32[]{:S(2)}) %copy-start) | copy-done | bytes 2097176
  65.5 0.0 copy-start.3
  65.5 1.2 copy-done.3
  66.7 0.0 copy-start.5
  66.7 0.8 copy-done.5
  67.5 0.0 copy-start.4
  67.5 42.1 %shard_map.155.done_ref = bf16[8,256,128]{2,1,0:T(8,128)(2,1)S(1)} custom-call(s32[8]{0:T(128)S(1)} %fusion.begin_ref, bf16[8,512,128]{2,1,0:T(8,128)(2,1)S(1)} %copy-done.3, bf16[8,1024,128]{2,1,0:T(8,128)(2,1)S(1)} %copy-done, f32[8,16,128]{2,1,0:T(8,128)S(1)} %copy-done.5), custom_call_target="tpu_custom_call" | custom-call | tf_op jit(solution)/shard_map/pallas_call | solution.py:621
  109.6 0.0 copy-done.1
  109.6 0.0 copy-done.2
  109.6 0.0 copy-done.4
  109.7 38.8 %shard_map.156 = bf16[256,2048]{1,0:T(8,128)(2,1)S(1)} custom-call(bf16[8,256,128]{2,1,0:T(8,128)(2,1)S(1)} %shard_map.155.done_ref, bf16[1024,256]{1,0:T(8,128)(2,1)S(1)} %copy-done.4, bf16[256,2048]{1,0:T(8,128)(2,1)S(1)} %copy-done.1, bf16[256,2048]{1,0:T(8,128)(2,1)S(1)} %copy-done.2), custom_call_target="tpu_custom_call" | custom-call | tf_op jit(solution)/shard_map/pallas_call | solution.py:532
  148.5 1.0 copy.21
  (1 shorter events, 0.0 us)
Async XLA Ops:
  4.2 105.4 %copy-start.1 = (bf16[256,2048]{1,0:T(8,128)(2,1)S(1)}, bf16[256,2048]{1,0:T(8,128)(2,1)}, u32[]{:S(2)}) copy-start(bf16[256,2048]{1,0:T(8,128)(2,1)} %attn_weight.1) | copy-start | bytes 3145732
  4.2 105.4 %copy-start.2 = (bf16[256,2048]{1,0:T(8,128)(2,1)S(1)}, bf16[256,2048]{1,0:T(8,128)(2,1)}, u32[]{:S(2)}) copy-start(bf16[256,2048]{1,0:T(8,128)(2,1)} %conv_weight.1) | copy-start | bytes 3145732
  63.9 1.6 %copy-start = (bf16[8,1024,128]{2,1,0:T(8,128)(2,1)S(1)}, bf16[8,1024,128]{2,1,0:T(8,128)(2,1)}, u32[]{:S(2)}) copy-start(bf16[8,1024,128]{2,1,0:T(8,128)(2,1)} %get-tuple-element.10.kv_ref) | copy-start | bytes 6291460
  65.5 1.2 copy-start.3
  66.7 0.8 copy-start.5
  67.5 42.1 %copy-start.4 = (bf16[1024,256]{1,0:T(8,128)(2,1)S(1)}, bf16[1024,256]{1,0:T(8,128)(2,1)}, u32[]{:S(2)}) copy-start(bf16[1024,256]{1,0:T(8,128)(2,1)} %get-tuple-element.12.conv_ref) | copy-start | bytes 1572868

commit v4 on v3

--- a/solution.py
+++ b/solution.py
@@ -28,9 +28,11 @@
 
 
 def front_kernel(
-    plan, tokens_ref, mix_ref, qkv_gain_ref, taps_ref, conv_gain_ref, side_ref, *refs
+    plan, tokens_ref, mix_ref, query_gain_ref, key_gain_ref, taps_ref, conv_gain_ref, side_ref, *refs
 ):
     sp_count, tp_count, head_count, head_dim, chunk = plan
+    query_gain = jnp.concatenate([query_gain_ref[...]] * plan[2], axis=1)
+    key_gain = jnp.concatenate([key_gain_ref[...]] * plan[2], axis=1)
     weight_refs = refs[:6]
     kv_out, query_out, side_out, conv_out = refs[6:10]
     (
@@ -185,9 +187,9 @@
             product = jnp.dot(scaled[...], weights[index], preferred_element_type=jnp.float32)
             return product * row_scale
 
-        keys = normed(project(1), qkv_gain_ref[1:2, :]).astype(jnp.bfloat16)
+        keys = normed(project(1), key_gain).astype(jnp.bfloat16)
         values = project(2).astype(jnp.bfloat16)
-        queries = normed(project(0), qkv_gain_ref[0:1, :]).astype(jnp.bfloat16)
+        queries = normed(project(0), query_gain).astype(jnp.bfloat16)
         queries = (queries.astype(jnp.float32) * head_dim ** (-0.5)).astype(jnp.bfloat16)
         for head in range(head_count):
             at = slice(head * head_dim, (head + 1) * head_dim)
@@ -324,7 +326,7 @@
         edge.wait_send()
 
 
-def front(tokens, mix_gain, qkv_gain, taps, conv_gain, sides, weights, head_dim, piece):
+def front(tokens, mix_gain, query_gain, key_gain, taps, conv_gain, sides, weights, head_dim, piece):
     sp_count = lax.axis_size("sp")
     tp_count = lax.axis_size("tp")
     rows, features = tokens.shape
@@ -346,7 +348,7 @@
             jax.ShapeDtypeStruct((sp_count,) + sides.shape[1:], sides.dtype),
             jax.ShapeDtypeStruct((rows, width), bf16),
         ),
-        in_specs=[vmem] * 6 + [pl.BlockSpec(memory_space=pl.ANY)] * 6,
+        in_specs=[vmem] * 7 + [pl.BlockSpec(memory_space=pl.ANY)] * 6,
         out_specs=(vmem,) * 4,
         scratch_shapes=[
             VMEM((6,) + weights[0].shape, bf16),
@@ -370,15 +372,15 @@
         compiler_params=pltpu.CompilerParams(
             collective_id=0, has_side_effects=True, vmem_limit_bytes=56 * 1024 * 1024
         ),
-    )(tokens, mix_gain, qkv_gain, taps, conv_gain, sides, *weights)
-
-
-def back_kernel(
-    plan, done_ref, conv_ref, attn_weight, conv_weight, out_ref, landed, attn, partial, keep,
-    mate_out, mate_in, link_out, link_in, send, recv, local, mate_ssem, mate_rsem, link_ssem,
-    link_rsem
+    )(tokens, mix_gain, query_gain, key_gain, taps, conv_gain, sides, *weights)
+
+
+def rear_kernel(
+    plan, query_ref, kv_ref, side_ref, conv_ref, attn_weight, conv_weight, out_ref, done, landed,
+    attn, partial, keep, mate_out, mate_in, link_out, link_in, send, recv, local, mate_ssem,
+    mate_rsem, link_ssem, link_rsem
 ):
-    sp_count, tp_count, head_dim, sub = plan
+    sp_count, tp_count, head_dim, piece, sub = plan
     sp = lax.axis_index("sp")
     tp = lax.axis_index("tp")
     core = lax.rem(tp, CORES)
@@ -387,12 +389,15 @@
     first = tp - core
     targets = sp_count // CORES
     rows, width = conv_ref.shape
-    half = done_ref.shape[1]
-    piece = 2 * half
     pieces = rows // piece
     share = pieces // CORES
     block_rows = rows // tp_count
-    subs = block_rows // sub
+    chunk = min(256, piece)
+    half = chunk // 2
+    tile = piece // 2
+    span = 256
+    phases = 2
+    subs = block_rows // phases // sub
     greet(
         [
             (lax.rem(sp + step, sp_count), first + lax.rem(core + other, CORES))
@@ -405,52 +410,130 @@
     home = sp // targets
     slot = lax.rem(sp, targets) * CORES + core
     home_here = home == core
-
-    def away(step):
-        source = lax.rem(sp + step, sp_count)
-        return mesh_copy(
-            done_ref.at[source], landed.at[slot], send.at[step], recv.at[slot],
-            (source, first + home),
-        )
-
-    for step in range(1, sp_count):
-        away(step).start()
-
-    @pl.when(home_here)
-    def _():
-        pltpu.make_async_copy(done_ref.at[sp], landed.at[slot], local).start()
-
-    @pl.when(jnp.logical_not(home_here))
-    def _():
-        away(0).start()
-
-    for number in range(rows // block_rows):
-        at = pl.ds(number * block_rows, block_rows)
-        partial[at, :] = jnp.dot(
-            conv_ref[at, :], conv_weight[...], preferred_element_type=jnp.float32
-        )
-
-    for index in range(targets * CORES):
-        giver = core * targets + index // CORES
-        here = jnp.logical_and(giver == sp, core == index % CORES)
-
-        @pl.when(here)
+    place_here = lax.rem(sp, share) * CORES + core
+    low = lax.broadcasted_iota(jnp.int32, (half, LANES), 1) < head_dim
+    gain = side_ref[0, rows // LANES : rows // LANES + 1, :head_dim]
+
+    def away(phase, source):
+        return mesh_copy(
+            done.at[phase, source], landed.at[phase, slot], send.at[phase, source],
+            recv.at[phase, slot], (source, first + home),
+        )
+
+    def stay(phase, source, index):
+        return pltpu.make_async_copy(
+            done.at[phase, source], landed.at[phase, index], local.at[phase]
+        )
+
+    def queries_of(phase, source, spot):
+        begin = pl.multiple_of(spot * tile, half)
+        parts = []
+        for number in range(piece // chunk):
+            pair = query_ref[source, pl.ds(begin + number * half, half), :].astype(jnp.float32)
+            if phase:
+                pair = pltpu.roll(pair, head_dim, 1)
+            parts.append(jnp.where(low, pair, 0.0))
+        return jnp.concatenate(parts, axis=0).astype(jnp.bfloat16)
+
+    def fold(phase, source, queries, carried, spot=None):
+        top, total = carried
+        new_top = top
+        scores = []
+        for start in range(0, rows, span):
+            gates = side_ref[source, start // LANES : (start + span) // LANES, :]
+            gate_row = jnp.concatenate(
+                [gates[row : row + 1, :] for row in range(span // LANES)], axis=1
+            )
+            part = lax.dot_general(
+                queries, kv_ref[source, start : start + span, :],
+                (((1,), (1,)), ((), ())), preferred_element_type=jnp.float32,
+            ) - gate_row
+            if spot is not None:
+                row = lax.broadcasted_iota(jnp.int32, part.shape, 0)
+                row = row // half * chunk + lax.rem(row, half) + phase * half + spot * piece
+                column = lax.broadcasted_iota(jnp.int32, part.shape, 1) + start
+                part = jnp.where(column <= row, part, -jnp.inf)
+            new_top = jnp.maximum(new_top, jnp.max(part, axis=1, keepdims=True))
+            scores.append(part)
+        total = total * jnp.exp(top - new_top)
+        for index, part in enumerate(scores):
+            weights = jnp.exp(part - new_top).astype(jnp.bfloat16)
+            total = total + jnp.dot(
+                weights, kv_ref[source, index * span : (index + 1) * span, :],
+                preferred_element_type=jnp.float32,
+            )
+        return new_top, total
+
+    def finish(phase, source, carried):
+        attended = carried[1][:, head_dim:]
+        scale = lax.rsqrt(jnp.mean(attended * attended, axis=1, keepdims=True) + NORM_EPSILON)
+        mixed = (attended * scale * gain).astype(jnp.bfloat16)
+        done[phase, source, :, :] = jnp.concatenate(
+            [mixed[: tile // 2], mixed[tile // 2 :]], axis=1
+        )
+        stays = jnp.logical_and(source == sp, home_here)
+
+        @pl.when(stays)
         def _():
-            pltpu.make_async_copy(done_ref.at[0], landed.at[index], local).wait()
-
-        @pl.when(jnp.logical_not(here))
+            stay(phase, source, slot).start()
+
+        @pl.when(jnp.logical_not(stays))
         def _():
-            mesh_copy(
-                done_ref.at[0], landed.at[index], send.at[0], recv.at[index], (sp, mate)
-            ).wait_recv()
-
-        head = index // (share * CORES)
-        place = index % (share * CORES)
-        spot = jnp.where(lax.rem(sp, 2) == 0, place, pieces - 1 - place)
-        start = pl.multiple_of(spot * piece, piece)
-        lanes = slice(head * head_dim, (head + 1) * head_dim)
-        attn[pl.ds(start, half), lanes] = landed[index, :, :head_dim]
-        attn[pl.ds(start + half, half), lanes] = landed[index, :, head_dim:]
+            away(phase, source).start()
+
+    def attend(phase):
+        def pair_of_sources(pair, _):
+            even, odd = 2 * pair, 2 * pair + 1
+            even_spot, odd_spot = place_here, pieces - 1 - place_here
+            even_queries = queries_of(phase, even, even_spot)
+            odd_queries = queries_of(phase, odd, odd_spot)
+            empty = (
+                jnp.full((tile, 1), -1e30, jnp.float32),
+                jnp.zeros((tile, LANES), jnp.float32),
+            )
+
+            def both(source, carried):
+                return (
+                    fold(phase, source, even_queries, carried[0]),
+                    fold(phase, source, odd_queries, carried[1]),
+                )
+
+            even_state, odd_state = lax.fori_loop(0, even, both, (empty, empty))
+            odd_state = fold(phase, even, odd_queries, odd_state)
+            even_state = fold(phase, even, even_queries, even_state, even_spot)
+            odd_state = fold(phase, odd, odd_queries, odd_state, odd_spot)
+            finish(phase, even, even_state)
+            finish(phase, odd, odd_state)
+            return 0
+
+        lax.fori_loop(0, sp_count // 2, pair_of_sources, 0)
+
+    def arrive(phase):
+        for index in range(targets * CORES):
+            giver = core * targets + index // CORES
+            here = jnp.logical_and(giver == sp, core == index % CORES)
+
+            @pl.when(here)
+            def _():
+                stay(phase, 0, index).wait()
+
+            @pl.when(jnp.logical_not(here))
+            def _():
+                mesh_copy(
+                    done.at[phase, 0], landed.at[phase, index], send.at[phase, 0],
+                    recv.at[phase, index], (sp, mate),
+                ).wait_recv()
+
+            head = index // (share * CORES)
+            place = index % (share * CORES)
+            spot = jnp.where(lax.rem(sp, 2) == 0, place, pieces - 1 - place)
+            lanes = slice(head * head_dim, (head + 1) * head_dim)
+            for side, at in enumerate((0, tile // 2)):
+                offset = at // half * chunk + phase * half + at % half
+                start = pl.multiple_of(spot * piece + offset, tile // 2)
+                attn[pl.ds(start, tile // 2), lanes] = landed[
+                    phase, index, :, side * head_dim : (side + 1) * head_dim
+                ]
 
     def product(block, number):
         at = pl.ds(pl.multiple_of(block * block_rows + number * sub, sub), sub)
@@ -482,60 +565,79 @@
         link_out[step - 1, at, :] = total.astype(jnp.bfloat16)
         across(step, number).start()
 
-    waiting = []
-    for step in list(range(1, chips)) + [0]:
-        for number in range(subs):
+    def spread(phase):
+        waiting = []
+        for step in list(range(1, chips)) + [0]:
+            for number in range(phase * subs, (phase + 1) * subs):
+                at = within(number)
+                theirs = lax.rem(mate + CORES * step, tp_count)
+                ours = lax.rem(tp + CORES * step, tp_count)
+                mate_out[step, at, :] = product(theirs, number).astype(jnp.bfloat16)
+                to_mate(step, number).start()
+                keep[step, at, :] = product(ours, number)
+                if waiting:
+                    joined(*waiting.pop())
+                if step:
+                    waiting.append((step, number))
+
+    def settle(phase):
+        for number in range(phase * subs, (phase + 1) * subs):
             at = within(number)
-            theirs = lax.rem(mate + CORES * step, tp_count)
-            ours = lax.rem(tp + CORES * step, tp_count)
-            mate_out[step, at, :] = product(theirs, number).astype(jnp.bfloat16)
-            to_mate(step, number).start()
-            keep[step, at, :] = product(ours, number)
-            if waiting:
-                joined(*waiting.pop())
-            if step:
-                waiting.append((step, number))
-    for number in range(subs):
-        at = within(number)
-        to_mate(0, number).wait_recv()
-        total = keep[0, at, :] + mate_in[0, at, :].astype(jnp.float32)
-        for step in range(1, chips):
-            across(step, number).wait_recv()
-            total = total + link_in[step - 1, at, :].astype(jnp.float32)
-        out_ref[at, :] = total.astype(jnp.bfloat16)
+            to_mate(0, number).wait_recv()
+            total = keep[0, at, :] + mate_in[0, at, :].astype(jnp.float32)
+            for step in range(1, chips):
+                across(step, number).wait_recv()
+                total = total + link_in[step - 1, at, :].astype(jnp.float32)
+            out_ref[at, :] = total.astype(jnp.bfloat16)
+
+    attend(0)
+    for number in range(tp_count):
+        at = pl.ds(number * block_rows, block_rows)
+        partial[at, :] = jnp.dot(
+            conv_ref[at, :], conv_weight[...], preferred_element_type=jnp.float32
+        )
+    arrive(0)
+    spread(0)
+    attend(1)
+    settle(0)
+    arrive(1)
+    spread(1)
+    settle(1)
     for step in range(chips):
-        for number in range(subs):
+        for number in range(phases * subs):
             to_mate(step, number).wait_send()
             if step:
                 across(step, number).wait_send()
-    for step in range(1, sp_count):
-        away(step).wait_send()
-
-    @pl.when(jnp.logical_not(home_here))
-    def _():
-        away(0).wait_send()
-
-
-def back(done, conv_mixed, attn_weight, conv_weight, head_dim):
+    for phase in range(phases):
+        for step in range(1, sp_count):
+            away(phase, lax.rem(sp + step, sp_count)).wait_send()
+
+        @pl.when(jnp.logical_not(home_here))
+        def _():
+            away(phase, sp).wait_send()
+
+
+def rear(queries, kv, sides, conv_mixed, attn_weight, conv_weight, head_dim, piece):
     sp_count = lax.axis_size("sp")
     tp_count = lax.axis_size("tp")
     chips = tp_count // CORES
     rows, width = conv_mixed.shape
     features = attn_weight.shape[1]
     block_rows = rows // tp_count
-    sub = min(64, block_rows)
+    sub = min(64, block_rows // 2)
     subs = block_rows // sub
     links = max(chips - 1, 1)
     bf16 = jnp.bfloat16
     dma = pltpu.SemaphoreType.DMA
     vmem = pl.BlockSpec(memory_space=VMEM)
     return pl.pallas_call(
-        functools.partial(back_kernel, (sp_count, tp_count, head_dim, sub)),
+        functools.partial(rear_kernel, (sp_count, tp_count, head_dim, piece, sub)),
         out_shape=jax.ShapeDtypeStruct((block_rows, features), bf16),
-        in_specs=[vmem] * 4,
+        in_specs=[vmem] * 6,
         out_specs=vmem,
         scratch_shapes=[
-            VMEM(done.shape, bf16),
+            VMEM((2, sp_count, piece // 4, LANES), bf16),
+            VMEM((2, sp_count, piece // 4, LANES), bf16),
             VMEM((rows, width), bf16),
             VMEM((rows, features), jnp.float32),
             VMEM((chips, block_rows, features), jnp.float32),
@@ -543,96 +645,13 @@
             VMEM((chips, block_rows, features), bf16),
             VMEM((links, block_rows, features), bf16),
             VMEM((links, block_rows, features), bf16),
-            dma((sp_count,)), dma((sp_count,)), dma,
+            dma((2, sp_count)), dma((2, sp_count)), dma((2,)),
             dma((chips, subs)), dma((chips, subs)), dma((links, subs)), dma((links, subs)),
         ],
         compiler_params=pltpu.CompilerParams(
-            collective_id=1, has_side_effects=True, vmem_limit_bytes=48 * 1024 * 1024
+            collective_id=1, has_side_effects=True, vmem_limit_bytes=56 * 1024 * 1024
         ),
-    )(done, conv_mixed, attn_weight, conv_weight)
-
-
-def attention_kernel(begin_ref, query_ref, kv_ref, side_ref, out_ref):
-    piece_rows = out_ref.shape[1] * 2
-    head_dim = LANES // 2
-    tile = min(256, piece_rows)
-    half = tile // 2
-    sub = 256
-    full = pl.program_id(0)
-    begin = pl.multiple_of(begin_ref[full], half)
-    rows = kv_ref.shape[1]
-    low = lax.broadcasted_iota(jnp.int32, (half, LANES), 1) < head_dim
-    tiles = []
-    for number in range(piece_rows // tile):
-        pair = query_ref[0, pl.ds(begin + number * half, half), :].astype(jnp.float32)
-        left = jnp.where(low, pair, 0.0)
-        right = jnp.where(low, pltpu.roll(pair, head_dim, 1), 0.0)
-        tiles.append(jnp.concatenate([left, right], axis=0).astype(jnp.bfloat16))
-
-    def fold(source, carried, masked):
-        results = []
-        for number, (top, total) in enumerate(carried):
-            scores = []
-            new_top = top
-            for start in range(0, rows, sub):
-                gates = side_ref[source, start // LANES : (start + sub) // LANES, :]
-                gate_row = jnp.concatenate(
-                    [gates[row : row + 1, :] for row in range(sub // LANES)], axis=1
-                )
-                part = lax.dot_general(
-                    tiles[number], kv_ref[source, start : start + sub, :],
-                    (((1,), (1,)), ((), ())), preferred_element_type=jnp.float32,
-                ) - gate_row
-                if masked:
-                    row = lax.broadcasted_iota(jnp.int32, part.shape, 0) + 2 * begin + number * tile
-                    column = lax.broadcasted_iota(jnp.int32, part.shape, 1) + start
-                    part = jnp.where(column <= row, part, -jnp.inf)
-                new_top = jnp.maximum(new_top, jnp.max(part, axis=1, keepdims=True))
-                scores.append(part)
-            total = total * jnp.exp(top - new_top)
-            for index, part in enumerate(scores):
-                weights = jnp.exp(part - new_top).astype(jnp.bfloat16)
-                total = total + jnp.dot(
-                    weights, kv_ref[source, index * sub : (index + 1) * sub, :],
-                    preferred_element_type=jnp.float32,
-                )
-            results.append((new_top, total))
-        return tuple(results)
-
-    carried = tuple(
-        (jnp.full((tile, 1), -1e30, jnp.float32), jnp.zeros((tile, LANES), jnp.float32))
-        for _ in tiles
-    )
-    carried = lax.fori_loop(0, full, lambda index, now: fold(index, now, False), carried)
-    carried = fold(full, carried, True)
-    gain = side_ref[0, rows // LANES : rows // LANES + 1, :head_dim]
-    mixed = []
-    for _, total in carried:
-        attended = total[:, head_dim:]
-        scale = lax.rsqrt(jnp.mean(attended * attended, axis=1, keepdims=True) + NORM_EPSILON)
-        mixed.append((attended * scale * gain).astype(jnp.bfloat16))
-    mixed = jnp.concatenate(mixed, axis=0)
-    middle = piece_rows // 2
-    out_ref[0] = jnp.concatenate([mixed[:middle], mixed[middle:]], axis=1)
-
-
-def attention(begins, queries, kv, sides, piece):
-    sp_count = queries.shape[0]
-    return pl.pallas_call(
-        attention_kernel,
-        grid_spec=pltpu.PrefetchScalarGridSpec(
-            num_scalar_prefetch=1,
-            grid=(sp_count,),
-            in_specs=[
-                pl.BlockSpec((1,) + queries.shape[1:], lambda i, n: (i, 0, 0)),
-                pl.BlockSpec(kv.shape, lambda i, n: (0, 0, 0)),
-                pl.BlockSpec(sides.shape, lambda i, n: (0, 0, 0)),
-            ],
-            out_specs=pl.BlockSpec((1, piece // 2, LANES), lambda i, n: (i, 0, 0)),
-        ),
-        out_shape=jax.ShapeDtypeStruct((sp_count, piece // 2, LANES), jnp.bfloat16),
-        compiler_params=pltpu.CompilerParams(vmem_limit_bytes=48 * 1024 * 1024),
-    )(begins, queries, kv, sides)
+    )(queries, kv, sides, conv_mixed, attn_weight, conv_weight)
 
 
 def per_device(
@@ -657,9 +676,7 @@
     head_dim = query_gain.shape[0]
     width = query_weight.shape[1]
     heads = width // head_dim
-    sp = lax.axis_index("sp")
     sp_count = lax.axis_size("sp")
-    core = lax.rem(lax.axis_index("tp"), CORES)
     share = sp_count // CORES // heads
     pieces = CORES * share
     piece = rows // pieces
@@ -668,11 +685,11 @@
         attn_out_gain.reshape(heads, 1, head_dim), ((0, 0), (0, 7), (0, LANES - head_dim))
     )
     sides = jnp.concatenate([gate_rows, gain_rows], axis=1)
-    qkv_gain = jnp.stack([jnp.tile(query_gain, heads), jnp.tile(key_gain, heads)])
     kv, queries, sides, conv_mixed = front(
         tokens,
         mix_gain.reshape(1, -1),
-        qkv_gain,
+        query_gain.reshape(1, -1),
+        key_gain.reshape(1, -1),
         conv_taps,
         conv_out_gain.reshape(1, -1),
         sides,
@@ -687,12 +704,9 @@
         head_dim,
         piece,
     )
-    place = lax.rem(sp, share) * CORES + core
-    source = jnp.arange(sp_count, dtype=jnp.int32)
-    spot = jnp.where(source % 2 == 0, place, pieces - 1 - place)
-    begins = (spot * (piece // 2)).astype(jnp.int32)
-    finished = attention(begins, queries, kv, sides, piece)
-    return back(finished, conv_mixed, attn_out_weight, conv_out_weight, head_dim)
+    return rear(
+        queries, kv, sides, conv_mixed, attn_out_weight, conv_out_weight, head_dim, piece
+    )
 
 
 def solution(mesh):

time: 151 us -> 135 us (0.89)
  Pallas kernels: 141 us -> 129 us
  local copies, waits for them, and re-layouts: 7.59 us -> 3.78 us
    pallas_call x2 -> x1, Pallas kernels: 80.9 us -> 69.1 us  [rear(): pl.pallas_call(functools.partial(rear_kernel, (sp_count, tp_count, head_d...]
    unnamed x14 -> x2, local copies, waits for them, and re-layouts: 5.35 us -> 3.02 us
where the time goes in v4:
time: 135 us; the launch traced here: 133 us
  Pallas kernels  129 us (96%)
  local copies, waits for them, and re-layouts  3.78 us (3%)
    pallas_call x1, Pallas kernels, rear(): pl.pallas_call(functools.partial(rear_kernel, (sp_count, tp_count, head_d...  69.1 us
    pallas_call x1, Pallas kernels, front(): pl.pallas_call(functools.partial(front_kernel, (sp_count, tp_count, heads...  59.7 us
    unnamed x2, local copies, waits for them, and re-layouts  3.02 us

profile of v4, /device:TPU:0, one launch (start us, length us, event | category | flops | bytes accessed | tf_op | source)
XLA Modules:
  0.0 133.2 jit_solution(15007771836863578959)
XLA Ops:
  0.0 0.8 reshape.23
  0.8 0.7 copy.19
  1.5 0.6 select_maximum_fusion.side_ref
  2.1 59.7 %shard_map.154 = (bf16[8,1024,128]{2,1,0:T(8,128)(2,1)}, bf16[8,512,128]{2,1,0:T(8,128)(2,1)}, f32[8,16,128]{2,1,0:T(8,128)}, bf16[1024,256]{1,0:T(8,128)(2,1)}) custom-call(bf16[1024,512]{1,0:T(8,128)(2,1)} %tokens_ref.1, f32[1,2048]{1,0:T(1,128)} %bitcast.11, f32[1,64]{1,0:T(1,128)} %bitcast.13, f32[1,64]{1,0:T(1,128)} %bitcast.14, f32[3,256]{1,0:T(4,128)} %taps_ref.1, ...), custom_call_target="tpu_custom_call" | custom-call | tf_op jit(solution)/shard_map/pallas_call | solution.py:343
  61.8 69.1 %shard_map.155 = bf16[256,2048]{1,0:T(8,128)(2,1)} custom-call(bf16[8,512,128]{2,1,0:T(8,128)(2,1)} %get-tuple-element.9.query_ref, bf16[8,1024,128]{2,1,0:T(8,128)(2,1)} %get-tuple-element.10.kv_ref, f32[8,16,128]{2,1,0:T(8,128)} %get-tuple-element.11.side_ref, bf16[1024,256]{1,0:T(8,128)(2,1)} %get-tuple-element.12.conv_ref, ...), custom_call_target="tpu_custom_call" | custom-call | tf_op jit(solution)/shard_map/pallas_call | solution.py:633
  130.9 2.3 %copy.21 = bf16[256,2048]{1,0:T(8,128)(2,1)} copy(bf16[256,2048]{1,0:T(8,128)(2,1)} %shard_map.155) | data formatting | bytes 2097152
